TPU v7x, 32 devices: a whole 2x2x4 slice. The times are simulated.
32 devices in a mesh: rep: 4 (over z), fs: 4 (over y, x), tp: 2 (over core).
Axes of the slice: x: 2, y: 2, z: 4, core: 2. Of those that a mesh axis runs over, the one named last changes fastest.
Arguments:
- inputs: bfloat16 [2048, 2048], P('rep', 'fs'), may hold values from -6 to 6
- w_gate: bfloat16 [2048, 3072], P('fs', 'tp'), may hold values from -0.125 to 0.125
- w_up: bfloat16 [2048, 3072], P('fs', 'tp'), may hold values from -0.125 to 0.125
- conv_taps: bfloat16 [3, 3072], P(None, 'tp'), may hold values from -3.5 to 3.5
- w_down: bfloat16 [3072, 2048], P('tp', 'fs'), may hold values from -0.109375 to 0.109375
- out_grad: bfloat16 [2048, 2048], P('rep', 'fs'), may hold values from -6 to 6
Outputs:
- in_grad: bfloat16 [2048, 2048], P(('rep', 'tp'), 'fs')
- grad_gate: float32 [2048, 3072], P('fs', 'tp')
- grad_up: float32 [2048, 3072], P('fs', 'tp')
- grad_down: float32 [3072, 2048], P('tp', 'fs')
- grad_taps: float32 [3, 3072], P(None, 'tp')
- rows_gate: float32 [2048], P('fs')
- rows_up: float32 [2048], P('fs')
- rows_down: float32 [3072], P('tp')
All inputs are finite; a program needn't handle non-finite values.
Results may differ from a plain program's by a relative error of at most 0.025.
Values may be sent and summed in bfloat16 or wider, within the bound.
A program may use at most 64 MiB of HBM per device.

v0:
```python
import functools

import jax
import jax.numpy as jnp
from jax import lax
from jax.experimental import pallas as pl
from jax.experimental.pallas import tpu as pltpu
from jax.sharding import PartitionSpec as P

KW = 3


def shift_down(values, lag_rows):
    if lag_rows == 0:
        return values
    padding = jnp.zeros_like(values[:lag_rows])
    return jnp.concatenate([padding, values[:-lag_rows]], axis=0)


def shift_up(values, lag_rows):
    if lag_rows == 0:
        return values
    padding = jnp.zeros_like(values[:lag_rows])
    return jnp.concatenate([values[lag_rows:], padding], axis=0)


def contract(left, right, left_dim, right_dim):
    return lax.dot_general(
        left, right, (((left_dim,), (right_dim,)), ((), ())), preferred_element_type=jnp.float32
    )


def row_norms(grad_gate, grad_up, grad_down):
    gate_rows = jnp.sum(grad_gate * grad_gate, axis=1)
    up_rows = jnp.sum(grad_up * grad_up, axis=1)
    down_rows = jnp.sum(grad_down * grad_down, axis=1)
    gate_rows, up_rows = lax.psum((gate_rows, up_rows), "tp")
    down_rows = lax.psum(down_rows, "fs")
    return (gate_rows, up_rows, down_rows)


def shards(inputs, w_gate, w_up, conv_taps, w_down, out_grad):
    tap_weights = conv_taps.astype(jnp.float32)
    gate_part = jnp.dot(inputs, w_gate, preferred_element_type=jnp.float32)
    up_part = jnp.dot(inputs, w_up, preferred_element_type=jnp.float32)
    act_part = contract(out_grad, w_down, 1, 1)
    gate_sum, up_sum, act_sum = (
        lax.psum(gate_part.astype(jnp.bfloat16), "fs").astype(jnp.float32),
        lax.psum(up_part.astype(jnp.bfloat16), "fs").astype(jnp.float32),
        lax.psum(act_part.astype(jnp.bfloat16), "fs").astype(jnp.float32),
    )
    gate_pre = gate_sum.astype(jnp.bfloat16)
    up_val = up_sum.astype(jnp.bfloat16)
    act_grad = act_sum.astype(jnp.bfloat16)
    gate_float = gate_pre.astype(jnp.float32)
    up_float = up_val.astype(jnp.float32)
    act_float = act_grad.astype(jnp.float32)
    shifted = [shift_down(gate_float, KW - 1 - tap_index) for tap_index in range(KW)]
    pre_act = tap_weights[0] * shifted[0]
    for tap_index in range(1, KW):
        pre_act = pre_act + tap_weights[tap_index] * shifted[tap_index]
    sigmoid_pre = jax.nn.sigmoid(pre_act)
    hidden = (pre_act * sigmoid_pre * up_float).astype(jnp.bfloat16)
    up_grad = (act_float * pre_act * sigmoid_pre).astype(jnp.bfloat16)
    pre_grad = act_float * up_float * sigmoid_pre * (1.0 + pre_act * (1.0 - sigmoid_pre))
    gate_acc = tap_weights[0] * shift_up(pre_grad, KW - 1)
    for tap_index in range(1, KW):
        gate_acc = gate_acc + tap_weights[tap_index] * shift_up(pre_grad, KW - 1 - tap_index)
    gate_grad = gate_acc.astype(jnp.bfloat16)
    gate_rows = gate_grad
    up_rows = up_grad
    in_grad = lax.psum_scatter(
        (contract(gate_rows, w_gate, 1, 1) + contract(up_rows, w_up, 1, 1)).astype(jnp.bfloat16),
        "tp",
        scatter_dimension=0,
        tiled=True,
    )
    grad_gate = contract(inputs, gate_grad, 0, 0)
    grad_up = contract(inputs, up_grad, 0, 0)
    grad_down = contract(hidden, out_grad, 0, 0)
    grad_taps = jnp.stack(
        [jnp.sum(shifted[tap_index] * pre_grad, axis=0) for tap_index in range(KW)]
    )
    grad_gate, grad_up, grad_down, grad_taps = (
        lax.psum(grad_gate.astype(jnp.bfloat16), "rep").astype(jnp.float32),
        lax.psum(grad_up.astype(jnp.bfloat16), "rep").astype(jnp.float32),
        lax.psum(grad_down.astype(jnp.bfloat16), "rep").astype(jnp.float32),
        lax.psum(grad_taps.astype(jnp.bfloat16), "rep").astype(jnp.float32),
    )
    gate_rows, up_rows, down_rows = row_norms(grad_gate, grad_up, grad_down)
    weight_grads = (grad_gate, grad_up, grad_down, grad_taps, gate_rows, up_rows, down_rows)
    grad_gate, grad_up, grad_down, grad_taps, gate_rows, up_rows, down_rows = weight_grads
    return (in_grad, grad_gate, grad_up, grad_down, grad_taps, gate_rows, up_rows, down_rows)


LANES = 128
CW = 256
HALO = 16
MID_LAG = 3
OUT_LAG = 18
MESH_ID = pl.DeviceIdType.MESH


def layer_kernel(
    n_rep, n_fs,
    x_ref, wg_ref, wu_ref, taps_ref, wd_ref, og_ref,
    in_grad_ref, down_ref, gate_ref, up_ref, taps_out_ref, rows_gate_ref, rows_up_ref, rows_down_ref,
    xt, send_part, recv_part, h_all, g_all, u_all, part, from_out, from_in, tot,
    acc, ig_send, ig_recv, tap_all, tap_out, tap_in, tap_sum, rows, rows_tp, rows_fs,
    rs_send, rs_recv, ag_send, ag_recv, a_send, out_recv, in_recv, b_send, loc_sem, misc,
):
    tok, feat = x_ref.shape
    cw = CW
    chunks = wg_ref.shape[1] // cw
    subs = feat // cw
    own_rows = tok // 2
    span = own_rows + HALO
    total_pieces = chunks * 3 * subs
    f32, bf16 = jnp.float32, jnp.bfloat16
    r = lax.axis_index("rep")
    f = lax.axis_index("fs")
    t = lax.axis_index("tp")
    half_rep = n_rep // 2
    is_left = r < half_rep
    toward = jnp.where(is_left, r + 1, r - 1)
    outward = jnp.where(is_left, r - 1, r + 1)
    is_end = jnp.logical_or(r == 0, r == n_rep - 1)
    not_end = jnp.logical_not(is_end)
    is_mid = jnp.logical_or(r == half_rep - 1, r == half_rep)
    not_mid = jnp.logical_not(is_mid)
    beside = f + 1 - 2 * lax.rem(f, 2)
    across = lax.rem(f + 2, 4)
    corner = lax.rem(beside + 2, 4)
    peers = [beside, across, corner]
    side = lax.rem(f, 2)
    top = f // 2
    own_cols = pl.ds(pl.multiple_of(side * LANES, LANES), LANES)
    own_toks = pl.ds(pl.multiple_of(top * own_rows, own_rows), own_rows)

    barrier = pltpu.get_barrier_semaphore()
    for k in range(n_fs - 1):
        pl.semaphore_signal(barrier, inc=1, device_id={"fs": peers[k]}, device_id_type=MESH_ID)
    pl.semaphore_signal(barrier, inc=1, device_id={"tp": 1 - t}, device_id_type=MESH_ID)
    pl.semaphore_signal(barrier, inc=1, device_id={"rep": toward}, device_id_type=MESH_ID)

    @pl.when(not_end)
    def _():
        pl.semaphore_signal(barrier, inc=1, device_id={"rep": outward}, device_id_type=MESH_ID)

    pl.semaphore_wait(barrier, n_fs + 1 + jnp.where(not_end, 1, 0))

    def remote(src, dst, send, recv, device):
        return pltpu.make_async_remote_copy(
            src_ref=src, dst_ref=dst, send_sem=send, recv_sem=recv,
            device_id=device, device_id_type=MESH_ID,
        )

    sent = []

    def rs_copy(c, tensor, k):
        s = (c * 3 + tensor) * (n_fs - 1) + k
        return remote(
            send_part.at[c, tensor, peers[k]], recv_part.at[c, tensor, k],
            rs_send.at[s], rs_recv.at[s], {"fs": peers[k]},
        )

    def reduce_start(c):
        cols = slice(c * cw, (c + 1) * cw)
        for tensor in range(3):
            if tensor == 0:
                value = jnp.dot(x_ref[...], wg_ref[:, cols], preferred_element_type=f32)
            elif tensor == 1:
                value = jnp.dot(x_ref[...], wu_ref[:, cols], preferred_element_type=f32)
            else:
                value = contract(og_ref[...], wd_ref[cols, :], 1, 1)
            value = value.astype(bf16)
            for g in range(n_fs):
                first = (g // 2) * (own_rows - HALO)
                lane = (g % 2) * LANES
                send_part[c, tensor, g] = value[first : first + span, lane : lane + LANES]
            for k in range(n_fs - 1):
                copy = rs_copy(c, tensor, k)
                copy.start()
                sent.append(copy)

    def reduced(c, tensor):
        value = send_part[c, tensor, f].astype(f32)
        for k in range(n_fs - 1):
            rs_copy(c, tensor, k).wait_recv()
            value = value + recv_part[c, tensor, k].astype(f32)
        return value.astype(bf16).astype(f32)

    def block(c, tensor, owner, part_of=None):
        col = lax.rem(owner, 2) * LANES
        row = (owner // 2) * own_rows
        if tensor == 0:
            size = LANES if part_of is None else LANES // 2
            start = col + (0 if part_of is None else part_of * size)
            return h_all.at[
                c, pl.ds(pl.multiple_of(start, size), size), pl.ds(pl.multiple_of(row, own_rows), own_rows)
            ]
        size = own_rows if part_of is None else own_rows // 2
        start = row + (0 if part_of is None else part_of * size)
        ref = g_all if tensor == 1 else u_all
        return ref.at[c, pl.ds(pl.multiple_of(start, size), size), pl.ds(pl.multiple_of(col, LANES), LANES)]

    def ag_copy(c, tensor, step, owner):
        s = (c * 3 + tensor) * 4
        if step == 0:
            ref, slot, target = block(c, tensor, owner), 0, beside
        elif step == 1:
            ref, slot, target = block(c, tensor, owner), 1, across
        elif step == 2:
            ref, slot, target = block(c, tensor, owner, 1), 2, beside
        else:
            ref, slot, target = block(c, tensor, owner, 0), 3, across
        return remote(ref, ref, ag_send.at[s + slot], ag_recv.at[s + slot], {"fs": target})

    def gather_start(c, tensor):
        for step in (0, 1):
            copy = ag_copy(c, tensor, step, f)
            copy.start()
            sent.append(copy)

    def forward(c, tensor):
        ag_copy(c, tensor, 0, beside).wait_recv()
        copy = ag_copy(c, tensor, 3, beside)
        copy.start()
        sent.append(copy)
        ag_copy(c, tensor, 1, across).wait_recv()
        copy = ag_copy(c, tensor, 2, across)
        copy.start()
        sent.append(copy)

    def gathered(c, tensor):
        ag_copy(c, tensor, 2, corner).wait_recv()
        ag_copy(c, tensor, 3, corner).wait_recv()

    def own(value):
        return jnp.where(top == 0, value[:own_rows], value[HALO:])

    row_ids = lax.broadcasted_iota(jnp.int32, (span, LANES), 0)

    def down(value, lag):
        if lag == 0:
            return value
        return jnp.where(row_ids >= lag, pltpu.roll(value, lag, 0), 0.0)

    def up(value, lag):
        if lag == 0:
            return value
        return jnp.where(row_ids < span - lag, pltpu.roll(value, span - lag, 0), 0.0)

    def elementwise(c):
        cols = pl.ds(pl.multiple_of(c * cw + side * LANES, LANES), LANES)
        weights = taps_ref[:, cols].astype(f32)
        gate = reduced(c, 0)
        pre = weights[0:1] * down(gate, KW - 1)
        for j in range(1, KW):
            pre = pre + weights[j : j + 1] * down(gate, KW - 1 - j)
        sig = 1.0 / (1.0 + jnp.exp(-pre))
        silu = pre * sig
        up_val = reduced(c, 1)
        h_all[c, own_cols, own_toks] = own(silu * up_val).T.astype(bf16)
        gather_start(c, 0)
        act = reduced(c, 2)
        pre_grad = act * up_val * sig * (1.0 + pre * (1.0 - sig))
        grad = weights[0:1] * up(pre_grad, KW - 1)
        for j in range(1, KW):
            grad = grad + weights[j : j + 1] * up(pre_grad, KW - 1 - j)
        g_all[c, own_toks, own_cols] = own(grad).astype(bf16)
        gather_start(c, 1)
        u_all[c, own_toks, own_cols] = own(act * silu).astype(bf16)
        gather_start(c, 2)
        for j in range(KW):
            tap_all[f, c * KW + j : c * KW + j + 1, :] = jnp.sum(
                own(down(gate, KW - 1 - j) * pre_grad), axis=0, keepdims=True
            )

    def part_copy(p):
        return remote(part.at[p], from_out.at[p], a_send.at[p], out_recv.at[p], {"rep": toward})

    def exchange_copy(p):
        return remote(part.at[p], from_in.at[p], a_send.at[p], in_recv.at[p], {"rep": toward})

    def total_copy(p, src):
        return remote(src.at[p], from_in.at[p], b_send.at[p], in_recv.at[p], {"rep": outward})

    def local_copy(p, src, tensor, wait):
        c = p // (3 * subs)
        q = p % subs
        along = pl.ds(pl.multiple_of(c * cw, cw), cw)
        inner = pl.ds(pl.multiple_of(q * cw, cw), cw)
        if tensor == 0:
            dst = down_ref.at[along, inner]
        elif tensor == 1:
            dst = gate_ref.at[inner, along]
        else:
            dst = up_ref.at[inner, along]
        copy = pltpu.make_async_copy(src.at[p], dst, loc_sem.at[p])
        if wait:
            copy.wait()
        else:
            copy.start()

    def store_out(p, src, wait=False):
        kind = (p // subs) % 3
        for tensor in range(3):
            @pl.when(kind == tensor)
            def _(tensor=tensor):
                local_copy(p, src, tensor, wait)

    def stage_a(p, value):
        @pl.when(not_end)
        def _():
            part_copy(p).wait_recv()
            part[p] = (value + from_out[p].astype(f32)).astype(bf16)

        @pl.when(is_end)
        def _():
            part[p] = value.astype(bf16)

        @pl.when(is_mid)
        def _():
            exchange_copy(p).start()

        @pl.when(not_mid)
        def _():
            part_copy(p).start()

    def norms(p, value):
        square = value * value
        lanes = square[:, :LANES]
        for g in range(1, square.shape[1] // LANES):
            lanes = lanes + square[:, g * LANES : (g + 1) * LANES]
        for i in range(cw // LANES):
            rows[pl.ds(p * (cw // LANES) + i, 1), :] = jnp.sum(
                lanes[i * LANES : (i + 1) * LANES].T, axis=0, keepdims=True
            )

    def stage_b_mid(p):
        exchange_copy(p).wait_recv()
        value = (part[p].astype(f32) + from_in[p].astype(f32)).astype(bf16)
        tot[p] = value

        @pl.when(not_end)
        def _():
            total_copy(p, tot).start()

        store_out(p, tot)
        norms(p, value.astype(f32))

    def stage_b_out(p):
        exchange_copy(p).wait_recv()

        @pl.when(not_end)
        def _():
            total_copy(p, from_in).start()

        store_out(p, from_in)
        norms(p, from_in[p].astype(f32))

    def stage_b(slot):
        @pl.when(jnp.logical_and(is_mid, jnp.logical_and(slot >= MID_LAG, slot < total_pieces + MID_LAG)))
        def _():
            stage_b_mid(slot - MID_LAG)

        @pl.when(jnp.logical_and(not_mid, slot >= OUT_LAG))
        def _():
            stage_b_out(slot - OUT_LAG)

    def segment(c, tensor):
        gathered(c, tensor)

        @pl.loop(0, subs)
        def _(q):
            p = (c * 3 + tensor) * subs + q
            if tensor == 0:
                value = jnp.dot(
                    h_all[c], og_ref[:, pl.ds(pl.multiple_of(q * cw, cw), cw)], preferred_element_type=f32
                )
            elif tensor == 1:
                value = jnp.dot(xt[q], g_all[c], preferred_element_type=f32)
            else:
                value = jnp.dot(xt[q], u_all[c], preferred_element_type=f32)
            stage_a(p, value)
            stage_b(p)

    def input_term(c):
        cols = slice(c * cw, (c + 1) * cw)
        term = contract(g_all[c], wg_ref[:, cols], 1, 1) + contract(u_all[c], wu_ref[:, cols], 1, 1)
        if c == 0:
            acc[...] = term
        else:
            acc[...] += term

    reduce_start(0)
    for q in range(subs):
        xt[q] = x_ref[:, q * cw : (q + 1) * cw].astype(f32).T.astype(bf16)
    elementwise(0)
    if chunks > 1:
        reduce_start(1)
    tap_peers = []

    def advance(c):
        if c < chunks:
            elementwise(c)
            if c + 1 < chunks:
                reduce_start(c + 1)
        else:
            for k in range(n_fs - 1):
                copy = remote(
                    tap_all.at[f], tap_all.at[f], misc.at[2 * k], misc.at[2 * k + 1], {"fs": peers[k]}
                )
                copy.start()
                tap_peers.append(copy)

    forward(0, 0)
    for c in range(chunks):
        if c > 0:
            advance(c + 1)
        segment(c, 0)
        if c == 0:
            forward(c, 1)
        segment(c, 1)
        if c == 0:
            forward(c, 2)
            advance(c + 1)
        segment(c, 2)
        if c + 1 < chunks:
            for tensor in range(3):
                forward(c + 1, tensor)
        input_term(c)

    m = 2 * (n_fs - 1)
    half = tok // 2
    ig_send[...] = acc[...].astype(bf16)
    ig_copy = remote(
        ig_send.at[pl.ds(pl.multiple_of((1 - t) * half, half), half)], ig_recv,
        misc.at[m], misc.at[m + 1], {"tp": 1 - t},
    )
    ig_copy.start()

    for copy in tap_peers:
        copy.wait()
    tap_part = remote(tap_all, tap_out, misc.at[m + 2], misc.at[m + 3], {"rep": toward})
    tap_exchange = remote(tap_all, tap_in, misc.at[m + 2], misc.at[m + 4], {"rep": toward})
    tap_total = remote(tap_sum, tap_in, misc.at[m + 5], misc.at[m + 4], {"rep": outward})

    @pl.when(not_end)
    def _():
        tap_part.wait_recv()
        tap_all[...] = tap_all[...] + tap_out[...]

    @pl.when(is_mid)
    def _():
        tap_exchange.start()

    @pl.when(not_mid)
    def _():
        tap_part.start()

    ig_copy.wait()
    in_grad_ref[...] = (
        ig_send[pl.ds(pl.multiple_of(t * half, half), half), :].astype(f32) + ig_recv[...].astype(f32)
    ).astype(bf16)

    @pl.loop(total_pieces, total_pieces + OUT_LAG)
    def _(slot):
        stage_b(slot)

    tap_exchange.wait_recv()

    @pl.when(is_mid)
    def _():
        tap_sum[...] = tap_all[...] + tap_in[...]

    @pl.when(not_mid)
    def _():
        tap_sum[...] = tap_in[...]

    @pl.when(not_end)
    def _():
        tap_total.start()

    rows_copies = [
        remote(rows, rows_tp, misc.at[m + 6], misc.at[m + 7], {"tp": 1 - t})
    ]
    for k in range(n_fs - 1):
        rows_copies.append(
            remote(rows, rows_fs.at[k], misc.at[m + 8 + 2 * k], misc.at[m + 9 + 2 * k], {"fs": peers[k]})
        )
    for copy in rows_copies:
        copy.start()

    for copy in sent:
        copy.wait_send()
    tap_part.wait_send()

    @pl.loop(0, total_pieces)
    def _(p):
        part_copy(p).wait_send()

        @pl.when(not_end)
        def _():
            total_copy(p, tot).wait_send()

        store_out(p, tot, True)

    for copy in rows_copies:
        copy.wait()
    per = cw // LANES
    for tensor, rows_ref in ((1, rows_gate_ref), (2, rows_up_ref)):
        for q in range(subs):
            for i in range(per):
                value = jnp.zeros((1, LANES), f32)
                for c in range(chunks):
                    at = ((c * 3 + tensor) * subs + q) * per + i
                    value = value + (rows[at : at + 1, :] + rows_tp[at : at + 1, :])
                lane = (q * per + i) * LANES
                rows_ref[:, lane : lane + LANES] = value
    for c in range(chunks):
        for i in range(per):
            value = jnp.zeros((1, LANES), f32)
            for q in range(subs):
                at = (c * 3 * subs + q) * per + i
                value = value + rows[at : at + 1, :]
                for k in range(n_fs - 1):
                    value = value + rows_fs[k, at : at + 1, :]
            lane = (c * per + i) * LANES
            rows_down_ref[:, lane : lane + LANES] = value
            for j in range(KW):
                at = c * KW + j
                taps_out_ref[j : j + 1, lane : lane + LANES] = (
                    tap_sum[i, at : at + 1, :] + tap_sum[i + 2, at : at + 1, :]
                )

    @pl.when(not_end)
    def _():
        tap_total.wait_send()


def fits(shape, inputs, w_gate):
    n_rep, n_fs, n_tp = shape["rep"], shape["fs"], shape["tp"]
    tok, feat = inputs.shape
    return (
        n_rep == 4 and n_fs == 4 and n_tp == 2 and feat == 2 * CW
        and w_gate.shape[1] % CW == 0 and w_gate.shape[1] <= 1536 and tok % LANES == 0 and tok <= 512
    )


def fused_shards(shape, inputs, w_gate, w_up, conv_taps, w_down, out_grad):
    if not fits(shape, inputs, w_gate):
        return shards(inputs, w_gate, w_up, conv_taps, w_down, out_grad)
    n_rep, n_fs = shape["rep"], shape["fs"]
    tok, feat = inputs.shape
    hid = w_gate.shape[1]
    cw = CW
    chunks = hid // cw
    subs = feat // cw
    pieces = chunks * 3 * subs
    bf16, f32 = jnp.bfloat16, jnp.float32
    vmem = pl.BlockSpec(memory_space=pltpu.VMEM)
    hops = chunks * 3 * (n_fs - 1)
    dma = pltpu.SemaphoreType.DMA
    in_grad, down, gate, up, taps, rows_gate, rows_up, rows_down = pl.pallas_call(
        functools.partial(layer_kernel, n_rep, n_fs),
        out_shape=(
            jax.ShapeDtypeStruct((tok // 2, feat), bf16),
            jax.ShapeDtypeStruct((hid, feat), bf16),
            jax.ShapeDtypeStruct((feat, hid), bf16),
            jax.ShapeDtypeStruct((feat, hid), bf16),
            jax.ShapeDtypeStruct((KW, hid), f32),
            jax.ShapeDtypeStruct((1, feat), f32),
            jax.ShapeDtypeStruct((1, feat), f32),
            jax.ShapeDtypeStruct((1, hid), f32),
        ),
        in_specs=[vmem] * 6,
        out_specs=(vmem,) + (pl.BlockSpec(memory_space=pl.ANY),) * 3 + (vmem,) * 4,
        scratch_shapes=[
            pltpu.VMEM((subs, cw, tok), bf16),
            pltpu.VMEM((chunks, 3, n_fs, tok // 2 + HALO, LANES), bf16),
            pltpu.VMEM((chunks, 3, n_fs - 1, tok // 2 + HALO, LANES), bf16),
            pltpu.VMEM((chunks, cw, tok), bf16),
            pltpu.VMEM((chunks, tok, cw), bf16),
            pltpu.VMEM((chunks, tok, cw), bf16),
            pltpu.VMEM((pieces, cw, cw), bf16),
            pltpu.VMEM((pieces, cw, cw), bf16),
            pltpu.VMEM((pieces, cw, cw), bf16),
            pltpu.VMEM((pieces, cw, cw), bf16),
            pltpu.VMEM((tok, feat), f32),
            pltpu.VMEM((tok, feat), bf16),
            pltpu.VMEM((tok // 2, feat), bf16),
            pltpu.VMEM((n_fs, chunks * KW, LANES), f32),
            pltpu.VMEM((n_fs, chunks * KW, LANES), f32),
            pltpu.VMEM((n_fs, chunks * KW, LANES), f32),
            pltpu.VMEM((n_fs, chunks * KW, LANES), f32),
            pltpu.VMEM((2 * pieces, LANES), f32),
            pltpu.VMEM((2 * pieces, LANES), f32),
            pltpu.VMEM((n_fs - 1, 2 * pieces, LANES), f32),
            dma((hops,)), dma((hops,)), dma((chunks * 12,)), dma((chunks * 12,)),
            dma((pieces,)), dma((pieces,)), dma((pieces,)), dma((pieces,)), dma((pieces,)),
            dma((4 * (n_fs - 1) + 8,)),
        ],
        compiler_params=pltpu.CompilerParams(
            collective_id=0, has_side_effects=True, vmem_limit_bytes=60 * 1024 * 1024
        ),
    )(inputs, w_gate, w_up, conv_taps, w_down, out_grad)
    return (
        in_grad, gate.astype(f32), up.astype(f32), down.astype(f32), taps,
        rows_gate.reshape(feat), rows_up.reshape(feat), rows_down.reshape(hid),
    )


def solution(mesh):
    return jax.shard_map(
        functools.partial(fused_shards, dict(mesh.shape)),
        mesh=mesh,
        in_specs=(
            P("rep", "fs"),
            P("fs", "tp"),
            P("fs", "tp"),
            P(None, "tp"),
            P("tp", "fs"),
            P("rep", "fs"),
        ),
        out_specs=(
            P(("rep", "tp"), "fs"),
            P("fs", "tp"),
            P("fs", "tp"),
            P("tp", "fs"),
            P(None, "tp"),
            P("fs"),
            P("fs"),
            P("tp"),
        ),
        check_vma=False,
    )
```

profile of v0, /device:TPU:0, one launch (start us, length us, event | category | flops | bytes accessed | tf_op | source)
XLA Modules:
  0.0 173.9 jit_solution(516012700803833928)
XLA Ops:
  0.6 162.3 %shard_map.125 = (bf16[256,512]{1,0:T(8,128)(2,1)}, bf16[1536,512]{1,0:T(8,128)(2,1)}, bf16[512,1536]{1,0:T(8,128)(2,1)}, bf16[512,1536]{1,0:T(8,128)(2,1)}, f32...) custom-call(bf16[512,512]{1,0:T(8,128)(2,1)} %x_ref.1, bf16[512,1536]{1,0:T(8,128)(2,1)} %wg_ref.1, ...), custom_call_target="tpu_custom_call" | custom-call | tf_op jit(solution)/shard_map/pallas_call | solution.py:566
  163.0 0.0 copy-start.1
  163.0 3.6 %convert_element_type.10 = f32[512,1536]{1,0:T(8,128)} convert(bf16[512,1536]{1,0:T(8,128)(2,1)} %get-tuple-element.18) | non-fusion elementwise | flops 786432 | bytes 4718592 | tf_op jit(solution)/shard_map/convert_element_type | solution.py:610
  166.6 0.0 copy-done.1
  166.6 0.0 copy-start
  166.6 2.1 %convert_element_type.11 = f32[1536,512]{1,0:T(8,128)} convert(bf16[1536,512]{1,0:T(8,128)(2,1)S(1)} %copy-done.1) | non-fusion elementwise | flops 786432 | bytes 4718592 | tf_op jit(solution)/shard_map/convert_element_type | solution.py:610
  168.7 0.0 copy-done
  168.7 0.0 copy-start.4
  168.7 0.0 copy-start.2
  168.7 0.0 copy-start.3
  168.7 0.0 copy-start.6
  168.7 0.0 copy-start.5
  168.7 2.1 %convert_element_type.9 = f32[512,1536]{1,0:T(8,128)} convert(bf16[512,1536]{1,0:T(8,128)(2,1)S(1)} %copy-done) | non-fusion elementwise | flops 786432 | bytes 4718592 | tf_op jit(solution)/shard_map/convert_element_type | solution.py:610
  170.8 0.0 copy-done.4
  170.8 0.6 reduce
  171.4 0.0 copy-done.2
  171.4 0.7 copy.18
  172.1 0.0 copy-done.3
  172.1 0.6 copy.19
  172.7 0.0 copy-done.6
  172.7 0.6 copy.20
  173.3 0.0 copy-done.5
  173.3 0.6 copy.21
Async XLA Ops:
  163.0 3.6 %copy-start.1 = (bf16[1536,512]{1,0:T(8,128)(2,1)S(1)}, bf16[1536,512]{1,0:T(8,128)(2,1)}, u32[]{:S(2)}) copy-start(bf16[1536,512]{1,0:T(8,128)(2,1)} %get-tuple-element.19) | copy-start | bytes 4718596
  166.6 2.1 %copy-start = (bf16[512,1536]{1,0:T(8,128)(2,1)S(1)}, bf16[512,1536]{1,0:T(8,128)(2,1)}, u32[]{:S(2)}) copy-start(bf16[512,1536]{1,0:T(8,128)(2,1)} %get-tuple-element.17) | copy-start | bytes 4718596
  168.7 2.1 %copy-start.4 = (f32[1,1536]{1,0:T(1,128)S(1)}, f32[1,1536]{1,0:T(1,128)}, u32[]{:S(2)}) copy-start(f32[1,1536]{1,0:T(1,128)} %get-tuple-element.23) | copy-start | bytes 18436
  168.7 2.7 %copy-start.2 = (bf16[256,512]{1,0:T(8,128)(2,1)S(1)}, bf16[256,512]{1,0:T(8,128)(2,1)}, u32[]{:S(2)}) copy-start(bf16[256,512]{1,0:T(8,128)(2,1)} %get-tuple-element.32) | copy-start | bytes 786436
  168.7 3.4 %copy-start.3 = (f32[3,1536]{1,0:T(4,128)S(1)}, f32[3,1536]{1,0:T(4,128)}, u32[]{:S(2)}) copy-start(f32[3,1536]{1,0:T(4,128)} %get-tuple-element.36) | copy-start | bytes 55300
  168.7 4.0 %copy-start.6 = (f32[1,512]{1,0:T(1,128)S(1)}, f32[1,512]{1,0:T(1,128)}, u32[]{:S(2)}) copy-start(f32[1,512]{1,0:T(1,128)} %get-tuple-element.21) | copy-start | bytes 6148
  168.7 4.6 %copy-start.5 = (f32[1,512]{1,0:T(1,128)S(1)}, f32[1,512]{1,0:T(1,128)}, u32[]{:S(2)}) copy-start(f32[1,512]{1,0:T(1,128)} %get-tuple-element.22) | copy-start | bytes 6148
where the time goes:
time: 174 us
  Pallas kernels  162 us (93%)
  other arithmetic  8.39 us (5%)
  local copies, waits for them, and re-layouts  2.5 us (1%)
    pallas_call x1, Pallas kernels, fused_shards(): pl.pallas_call(functools.partial(layer_kernel, n_rep, n_fs), out_shape=(j...  162 us
    convert_element_type x1, other arithmetic, fused_shards(): up.astype(f32)  3.6 us

commit v1 on v0

v1 whole, which is shorter than its diff:
```python
import functools

import jax
import jax.numpy as jnp
from jax import lax
from jax.experimental import pallas as pl
from jax.experimental.pallas import tpu as pltpu
from jax.sharding import PartitionSpec as P

KW = 3


def shift_down(values, lag_rows):
    if lag_rows == 0:
        return values
    padding = jnp.zeros_like(values[:lag_rows])
    return jnp.concatenate([padding, values[:-lag_rows]], axis=0)


def shift_up(values, lag_rows):
    if lag_rows == 0:
        return values
    padding = jnp.zeros_like(values[:lag_rows])
    return jnp.concatenate([values[lag_rows:], padding], axis=0)


def contract(left, right, left_dim, right_dim):
    return lax.dot_general(
        left, right, (((left_dim,), (right_dim,)), ((), ())), preferred_element_type=jnp.float32
    )


def row_norms(grad_gate, grad_up, grad_down):
    gate_rows = jnp.sum(grad_gate * grad_gate, axis=1)
    up_rows = jnp.sum(grad_up * grad_up, axis=1)
    down_rows = jnp.sum(grad_down * grad_down, axis=1)
    gate_rows, up_rows = lax.psum((gate_rows, up_rows), "tp")
    down_rows = lax.psum(down_rows, "fs")
    return (gate_rows, up_rows, down_rows)


def shards(inputs, w_gate, w_up, conv_taps, w_down, out_grad):
    tap_weights = conv_taps.astype(jnp.float32)
    gate_part = jnp.dot(inputs, w_gate, preferred_element_type=jnp.float32)
    up_part = jnp.dot(inputs, w_up, preferred_element_type=jnp.float32)
    act_part = contract(out_grad, w_down, 1, 1)
    gate_sum, up_sum, act_sum = (
        lax.psum(gate_part.astype(jnp.bfloat16), "fs").astype(jnp.float32),
        lax.psum(up_part.astype(jnp.bfloat16), "fs").astype(jnp.float32),
        lax.psum(act_part.astype(jnp.bfloat16), "fs").astype(jnp.float32),
    )
    gate_pre = gate_sum.astype(jnp.bfloat16)
    up_val = up_sum.astype(jnp.bfloat16)
    act_grad = act_sum.astype(jnp.bfloat16)
    gate_float = gate_pre.astype(jnp.float32)
    up_float = up_val.astype(jnp.float32)
    act_float = act_grad.astype(jnp.float32)
    shifted = [shift_down(gate_float, KW - 1 - tap_index) for tap_index in range(KW)]
    pre_act = tap_weights[0] * shifted[0]
    for tap_index in range(1, KW):
        pre_act = pre_act + tap_weights[tap_index] * shifted[tap_index]
    sigmoid_pre = jax.nn.sigmoid(pre_act)
    hidden = (pre_act * sigmoid_pre * up_float).astype(jnp.bfloat16)
    up_grad = (act_float * pre_act * sigmoid_pre).astype(jnp.bfloat16)
    pre_grad = act_float * up_float * sigmoid_pre * (1.0 + pre_act * (1.0 - sigmoid_pre))
    gate_acc = tap_weights[0] * shift_up(pre_grad, KW - 1)
    for tap_index in range(1, KW):
        gate_acc = gate_acc + tap_weights[tap_index] * shift_up(pre_grad, KW - 1 - tap_index)
    gate_grad = gate_acc.astype(jnp.bfloat16)
    gate_rows = gate_grad
    up_rows = up_grad
    in_grad = lax.psum_scatter(
        (contract(gate_rows, w_gate, 1, 1) + contract(up_rows, w_up, 1, 1)).astype(jnp.bfloat16),
        "tp",
        scatter_dimension=0,
        tiled=True,
    )
    grad_gate = contract(inputs, gate_grad, 0, 0)
    grad_up = contract(inputs, up_grad, 0, 0)
    grad_down = contract(hidden, out_grad, 0, 0)
    grad_taps = jnp.stack(
        [jnp.sum(shifted[tap_index] * pre_grad, axis=0) for tap_index in range(KW)]
    )
    grad_gate, grad_up, grad_down, grad_taps = (
        lax.psum(grad_gate.astype(jnp.bfloat16), "rep").astype(jnp.float32),
        lax.psum(grad_up.astype(jnp.bfloat16), "rep").astype(jnp.float32),
        lax.psum(grad_down.astype(jnp.bfloat16), "rep").astype(jnp.float32),
        lax.psum(grad_taps.astype(jnp.bfloat16), "rep").astype(jnp.float32),
    )
    gate_rows, up_rows, down_rows = row_norms(grad_gate, grad_up, grad_down)
    weight_grads = (grad_gate, grad_up, grad_down, grad_taps, gate_rows, up_rows, down_rows)
    grad_gate, grad_up, grad_down, grad_taps, gate_rows, up_rows, down_rows = weight_grads
    return (in_grad, grad_gate, grad_up, grad_down, grad_taps, gate_rows, up_rows, down_rows)


LANES = 128
CW = 256
HALO = 16
A_LAG = 2
B_LAG = 4
OUT_LAG = 10
RING = 4
MESH_ID = pl.DeviceIdType.MESH

STEPS = (
    (),
    (("forward", 0, 1), ("reduce", 1, 1)),
    (("forward", 0, 2),),
    (("reduce", 1, 2),),
    (("hidden", 1, 0),),
    (("grads", 1, 0), ("forward", 1, 0), ("gather", 1, 1), ("gather", 1, 2), ("reduce", 2, 0)),
)


def layer_kernel(
    n_rep, n_fs,
    x_hbm, wg_hbm, wu_hbm, taps_ref, wd_hbm, og_hbm,
    in_grad_ref, down_ref, gate_ref, up_ref, taps_out_ref, rows_gu_ref, rows_down_ref,
    x_ref, wg_ref, wu_ref, wd_ref, og_ref,
    xt, send_part, recv_part, held, h_all, g_all, u_all, ring, part, from_out, from_in, tot,
    acc, ig_send, ig_recv, tap_all, tap_two, tap_out, tap_in, tap_sum, rows_gu, rows_d, rows_tp, rows_fs,
    rs_send, rs_recv, ag_send, ag_recv, a_send, out_recv, in_recv, b_send, loc_sem, misc,
):
    tok, feat = x_ref.shape
    cw = CW
    chunks = wg_ref.shape[1] // cw
    subs = feat // cw
    own_rows = tok // 2
    span = own_rows + HALO
    slots = 3 * subs
    total_pieces = chunks * slots
    per = cw // LANES
    f32, bf16 = jnp.float32, jnp.bfloat16
    r = lax.axis_index("rep")
    f = lax.axis_index("fs")
    t = lax.axis_index("tp")
    half_rep = n_rep // 2
    is_left = r < half_rep
    toward = jnp.where(is_left, r + 1, r - 1)
    outward = jnp.where(is_left, r - 1, r + 1)
    is_end = jnp.logical_or(r == 0, r == n_rep - 1)
    is_mid = jnp.logical_not(is_end)
    beside = f + 1 - 2 * lax.rem(f, 2)
    across = lax.rem(f + 2, 4)
    corner = lax.rem(beside + 2, 4)
    peers = [beside, across, corner]
    side = lax.rem(f, 2)
    top = f // 2
    own_cols = pl.ds(pl.multiple_of(side * LANES, LANES), LANES)
    own_toks = pl.ds(pl.multiple_of(top * own_rows, own_rows), own_rows)

    barrier = pltpu.get_barrier_semaphore()
    for k in range(n_fs - 1):
        pl.semaphore_signal(barrier, inc=1, device_id={"fs": peers[k]}, device_id_type=MESH_ID)
    pl.semaphore_signal(barrier, inc=1, device_id={"tp": 1 - t}, device_id_type=MESH_ID)
    pl.semaphore_signal(barrier, inc=1, device_id={"rep": toward}, device_id_type=MESH_ID)

    @pl.when(is_mid)
    def _():
        pl.semaphore_signal(barrier, inc=1, device_id={"rep": outward}, device_id_type=MESH_ID)

    loads = []

    def load(src, dst):
        copy = pltpu.make_async_copy(src, dst, loc_sem.at[len(loads)])
        copy.start()
        loads.append(copy)

    first = slice(0, cw)
    load(x_hbm, x_ref)
    load(wg_hbm.at[:, first], wg_ref.at[:, first])
    load(wu_hbm.at[:, first], wu_ref.at[:, first])
    load(og_hbm, og_ref)
    load(wd_hbm.at[first], wd_ref.at[first])
    if chunks > 1:
        rest = slice(cw, chunks * cw)
        load(wg_hbm.at[:, rest], wg_ref.at[:, rest])
        load(wu_hbm.at[:, rest], wu_ref.at[:, rest])
        load(wd_hbm.at[rest], wd_ref.at[rest])

    def remote(src, dst, send, recv, device):
        return pltpu.make_async_remote_copy(
            src_ref=src, dst_ref=dst, send_sem=send, recv_sem=recv,
            device_id=device, device_id_type=MESH_ID,
        )

    def chunk_cols(c):
        if isinstance(c, int):
            return slice(c * cw, (c + 1) * cw)
        return pl.ds(pl.multiple_of(c * cw, cw), cw)

    def rs_copy(c, tensor, k):
        s = (c * 3 + tensor) * (n_fs - 1) + k
        return remote(
            send_part.at[c, tensor, peers[k]], recv_part.at[c, tensor, k],
            rs_send.at[s], rs_recv.at[s], {"fs": peers[k]},
        )

    def product(c, tensor):
        cols = chunk_cols(c)
        if tensor == 0:
            value = jnp.dot(x_ref[...], wg_ref[:, cols], preferred_element_type=f32)
        elif tensor == 1:
            value = jnp.dot(x_ref[...], wu_ref[:, cols], preferred_element_type=f32)
        else:
            value = contract(og_ref[...], wd_ref[cols, :], 1, 1)
        value = value.astype(bf16)
        for g in range(n_fs):
            row = (g // 2) * (own_rows - HALO)
            lane = (g % 2) * LANES
            send_part[c, tensor, g] = value[row : row + span, lane : lane + LANES]

    def reduce_send(c, tensor):
        for k in range(n_fs - 1):
            rs_copy(c, tensor, k).start()

    def reduce_start(c, tensor):
        product(c, tensor)
        reduce_send(c, tensor)

    def reduced(c, tensor):
        value = send_part[c, tensor, f].astype(f32)
        for k in range(n_fs - 1):
            rs_copy(c, tensor, k).wait_recv()
            value = value + recv_part[c, tensor, k].astype(f32)
        return value.astype(bf16).astype(f32)

    def block(c, tensor, owner, part_of=None):
        col = lax.rem(owner, 2) * LANES
        row = (owner // 2) * own_rows
        if tensor == 0:
            size = LANES if part_of is None else LANES // 2
            start = col + (0 if part_of is None else part_of * size)
            return h_all.at[
                c, pl.ds(pl.multiple_of(start, size), size), pl.ds(pl.multiple_of(row, own_rows), own_rows)
            ]
        size = own_rows if part_of is None else own_rows // 2
        start = row + (0 if part_of is None else part_of * size)
        ref = g_all if tensor == 1 else u_all
        return ref.at[c, pl.ds(pl.multiple_of(start, size), size), pl.ds(pl.multiple_of(col, LANES), LANES)]

    def ag_copy(c, tensor, step, owner):
        s = (c * 3 + tensor) * 4
        if step == 0:
            ref, slot, target = block(c, tensor, owner), 0, beside
        elif step == 1:
            ref, slot, target = block(c, tensor, owner), 1, across
        elif step == 2:
            ref, slot, target = block(c, tensor, owner, 1), 2, beside
        else:
            ref, slot, target = block(c, tensor, owner, 0), 3, across
        return remote(ref, ref, ag_send.at[s + slot], ag_recv.at[s + slot], {"fs": target})

    def gather_start(c, tensor):
        for step in (0, 1):
            ag_copy(c, tensor, step, f).start()

    def forward(c, tensor):
        ag_copy(c, tensor, 0, beside).wait_recv()
        ag_copy(c, tensor, 3, beside).start()
        ag_copy(c, tensor, 1, across).wait_recv()
        ag_copy(c, tensor, 2, across).start()

    def gathered(c, tensor):
        ag_copy(c, tensor, 2, corner).wait_recv()
        ag_copy(c, tensor, 3, corner).wait_recv()

    def own(value):
        return jnp.where(top == 0, value[:own_rows], value[HALO:])

    row_ids = lax.broadcasted_iota(jnp.int32, (span, LANES), 0)

    def down(value, lag):
        if lag == 0:
            return value
        return jnp.where(row_ids >= lag, pltpu.roll(value, lag, 0), 0.0)

    def up(value, lag):
        if lag == 0:
            return value
        return jnp.where(row_ids < span - lag, pltpu.roll(value, span - lag, 0), 0.0)

    def own_weights(c):
        cols = pl.ds(pl.multiple_of(c * cw + side * LANES, LANES), LANES)
        return taps_ref[:, cols].astype(f32)

    def hidden_step(c):
        weights = own_weights(c)
        gate = reduced(c, 0)
        pre = weights[0:1] * down(gate, KW - 1)
        for j in range(1, KW):
            pre = pre + weights[j : j + 1] * down(gate, KW - 1 - j)
        sig = 1.0 / (1.0 + jnp.exp(-pre))
        up_val = reduced(c, 1)
        h_all[c, own_cols, own_toks] = own(pre * sig * up_val).T.astype(bf16)
        gather_start(c, 0)
        held[0] = gate
        held[1] = up_val
        held[2] = pre
        held[3] = sig

    def grads_step(c):
        weights = own_weights(c)
        gate, up_val, pre, sig = held[0], held[1], held[2], held[3]
        act = reduced(c, 2)
        pre_grad = act * up_val * sig * (1.0 + pre * (1.0 - sig))
        grad = weights[0:1] * up(pre_grad, KW - 1)
        for j in range(1, KW):
            grad = grad + weights[j : j + 1] * up(pre_grad, KW - 1 - j)
        g_all[c, own_toks, own_cols] = own(grad).astype(bf16)
        u_all[c, own_toks, own_cols] = own(act * (pre * sig)).astype(bf16)
        for j in range(KW):
            tap_all[f, pl.ds(c * KW + j, 1), :] = jnp.sum(
                own(down(gate, KW - 1 - j) * pre_grad), axis=0, keepdims=True
            )

    def part_copy(p):
        return remote(part.at[p], from_out.at[p], a_send.at[p], out_recv.at[p], {"rep": toward})

    def exchange_copy(p):
        return remote(part.at[p], from_in.at[p], a_send.at[p], in_recv.at[p], {"rep": toward})

    def total_copy(p, src):
        return remote(src.at[p], from_in.at[p], b_send.at[p], in_recv.at[p], {"rep": outward})

    def finished(c, s, value):
        tensor, q = s // subs, s % subs
        inner = slice(q * cw, (q + 1) * cw)
        if tensor == 0:
            down_ref[chunk_cols(c), inner] = value
        elif tensor == 1:
            gate_ref[inner, chunk_cols(c)] = value
        else:
            up_ref[inner, chunk_cols(c)] = value
        value = value.astype(f32)
        square = value * value
        lanes = square[:, :LANES]
        for g in range(1, cw // LANES):
            lanes = lanes + square[:, g * LANES : (g + 1) * LANES]
        for i in range(per):
            row = jnp.sum(lanes[i * LANES : (i + 1) * LANES].T, axis=0, keepdims=True)
            if tensor == 0:
                at = pl.ds(c * per + i, 1)
                rows_d[at, :] = row if q == 0 else rows_d[at, :] + row
            else:
                at = ((tensor - 1) * subs + q) * per + i
                rows_gu[at : at + 1, :] = rows_gu[at : at + 1, :] + row

    def stage_a(p):
        part_copy(p).wait_recv()
        part[p] = (ring[lax.rem(p, RING)] + from_out[p].astype(f32)).astype(bf16)
        exchange_copy(p).start()

    def stage_b(c, s):
        p = c * slots + s
        exchange_copy(p).wait_recv()
        value = (part[p].astype(f32) + from_in[p].astype(f32)).astype(bf16)
        tot[p] = value
        total_copy(p, tot).start()
        finished(c, s, value)

    def stage_out(c, s):
        exchange_copy(c * slots + s).wait_recv()
        finished(c, s, from_in[c * slots + s])

    def behind(c, s, lag):
        back = (lag - s + slots - 1) // slots if lag > s else 0
        return c - back, s - lag + back * slots, back

    def guarded(c, lowest, fn):
        if isinstance(c, int):
            if c >= lowest:
                fn()
        elif lowest <= 1:
            fn()
        else:
            pl.when(c >= lowest)(fn)

    def work(c, s):
        tensor, q = s // subs, s % subs
        p = c * slots + s
        if q == 0:
            gathered(c, tensor)
        if tensor == 0:
            value = jnp.dot(h_all[c], og_ref[:, q * cw : (q + 1) * cw], preferred_element_type=f32)
        elif tensor == 1:
            value = jnp.dot(xt[q], g_all[c], preferred_element_type=f32)
        else:
            value = jnp.dot(xt[q], u_all[c], preferred_element_type=f32)
        ca, sa, ka = behind(c, s, A_LAG)
        cb, sb, kb = behind(c, s, B_LAG)
        co, so, ko = behind(c, s, OUT_LAG)

        @pl.when(is_end)
        def _():
            part[p] = value.astype(bf16)
            part_copy(p).start()
            guarded(c, ko, lambda: stage_out(co, so))

        @pl.when(is_mid)
        def _():
            ring[lax.rem(p, RING)] = value
            guarded(c, ka, lambda: stage_a(ca * slots + sa))
            guarded(c, kb, lambda: stage_b(cb, sb))

    def input_term(c):
        cols = chunk_cols(c)
        term = contract(g_all[c], wg_ref[:, cols], 1, 1) + contract(u_all[c], wu_ref[:, cols], 1, 1)
        if isinstance(c, int) and c == 0:
            acc[...] = term
        else:
            acc[...] += term

    actions = {
        "forward": forward,
        "reduce": reduce_start,
        "hidden": lambda c, tensor: hidden_step(c),
        "grads": lambda c, tensor: grads_step(c),
        "gather": gather_start,
    }

    def run(step, c):
        name, ahead, tensor = step
        target = c + ahead
        if isinstance(c, int):
            if target < chunks:
                actions[name](target, tensor)
        elif ahead == 0:
            actions[name](target, tensor)
        else:
            pl.when(target < chunks)(lambda: actions[name](target, tensor))

    def body(c):
        for s in range(slots):
            for step in STEPS[s]:
                run(step, c)
            work(c, s)
        input_term(c)

    loads[0].wait()
    loads[1].wait()
    product(0, 0)
    loads[2].wait()
    product(0, 1)
    pl.semaphore_wait(barrier, n_fs + 1 + jnp.where(is_mid, 1, 0))
    reduce_send(0, 0)
    reduce_send(0, 1)
    loads[3].wait()
    loads[4].wait()
    reduce_start(0, 2)
    for q in range(subs):
        xt[q] = x_ref[:, q * cw : (q + 1) * cw].astype(f32).T.astype(bf16)
    rows_gu[...] = jnp.zeros_like(rows_gu)
    for copy in loads[5:]:
        copy.wait()
    hidden_step(0)
    grads_step(0)
    forward(0, 0)
    gather_start(0, 1)
    gather_start(0, 2)
    if chunks > 1:
        reduce_start(1, 0)
    body(0)

    @pl.loop(1, chunks)
    def _(c):
        body(c)

    m = 2 * (n_fs - 1)
    half = tok // 2
    ig_send[...] = acc[...].astype(bf16)
    ig_copy = remote(
        ig_send.at[pl.ds(pl.multiple_of((1 - t) * half, half), half)], ig_recv,
        misc.at[m], misc.at[m + 1], {"tp": 1 - t},
    )
    ig_copy.start()

    tap_peers = []
    for k in range(n_fs - 1):
        tap_peers.append(remote(
            tap_all.at[f], tap_all.at[f], misc.at[2 * k], misc.at[2 * k + 1], {"fs": peers[k]}
        ))
        tap_peers[k].start()
    tap_part = remote(tap_two, tap_out, misc.at[m + 2], misc.at[m + 3], {"rep": toward})
    tap_exchange = remote(tap_two, tap_in, misc.at[m + 2], misc.at[m + 4], {"rep": toward})
    tap_total = remote(tap_sum, tap_in, misc.at[m + 5], misc.at[m + 4], {"rep": outward})

    def tap_first():
        for copy in tap_peers:
            copy.wait()
        for i in range(per):
            tap_two[i] = tap_all[i] + tap_all[i + 2]

    def input_finish():
        ig_copy.wait()
        in_grad_ref[...] = (
            ig_send[pl.ds(pl.multiple_of(t * half, half), half), :].astype(f32) + ig_recv[...].astype(f32)
        ).astype(bf16)

    fs_rows = [
        remote(rows_d, rows_fs.at[k], misc.at[m + 8 + 2 * k], misc.at[m + 9 + 2 * k], {"fs": peers[k]})
        for k in range(n_fs - 1)
    ]
    tp_rows = remote(rows_gu, rows_tp, misc.at[m + 6], misc.at[m + 7], {"tp": 1 - t})

    def rows_done(p, lag):
        if p == total_pieces - min(lag, slots - subs + 1):
            for copy in fs_rows:
                copy.start()
        if p == total_pieces - 1:
            tp_rows.start()

    @pl.when(is_end)
    def _():
        tap_first()
        tap_part.start()
        input_finish()
        for p in range(total_pieces - OUT_LAG, total_pieces):
            stage_out(p // slots, p % slots)
            rows_done(p, OUT_LAG)
        tap_exchange.wait_recv()
        tap_sum[...] = tap_in[...]

    @pl.when(is_mid)
    def _():
        for s in range(total_pieces, total_pieces + B_LAG):
            if s - A_LAG < total_pieces:
                stage_a(s - A_LAG)
            if s == total_pieces:
                tap_first()
            if s == total_pieces + A_LAG:
                tap_part.wait_recv()
                tap_two[...] = tap_two[...] + tap_out[...]
                tap_exchange.start()
                input_finish()
            stage_b((s - B_LAG) // slots, (s - B_LAG) % slots)
            rows_done(s - B_LAG, B_LAG)
        tap_exchange.wait_recv()
        tap_sum[...] = tap_two[...] + tap_in[...]
        tap_total.start()

    for c in range(chunks):
        for i in range(per):
            lane = (c * per + i) * LANES
            taps_out_ref[:, lane : lane + LANES] = tap_sum[i, c * KW : (c + 1) * KW, :]

    @pl.loop(0, chunks * 3)
    def _(n):
        c, tensor = n // 3, lax.rem(n, 3)
        for k in range(n_fs - 1):
            rs_copy(c, tensor, k).wait_send()
        for step, owner in ((0, f), (1, f), (2, across), (3, beside)):
            s = n * 4
            size = own_rows if step < 2 else own_rows // 2
            ref = g_all.at[c, pl.ds(0, size), pl.ds(0, LANES)]
            remote(ref, ref, ag_send.at[s + step], ag_recv.at[s + step], {"fs": beside}).wait_send()

    tap_part.wait_send()

    @pl.loop(0, total_pieces)
    def _(p):
        part_copy(p).wait_send()

        @pl.when(is_mid)
        def _():
            total_copy(p, tot).wait_send()

    for copy in fs_rows:
        copy.wait()
    rows_down_ref[...] = rows_d[...] + (rows_fs[0] + rows_fs[1] + rows_fs[2])
    tp_rows.wait()
    rows_gu_ref[...] = rows_gu[...] + rows_tp[...]

    @pl.when(is_mid)
    def _():
        tap_total.wait_send()


def finish_kernel(
    gate, up, down, in_grad, taps, rows_gu, rows_d,
    gate_out, up_out, down_out, in_grad_out, taps_out, rows_gate_out, rows_up_out, rows_down_out,
    wide_gate, wide_up, wide_down, sems,
):
    rows = CW
    copies = []
    for src, wide, dst in ((gate, wide_gate, gate_out), (up, wide_up, up_out), (down, wide_down, down_out)):
        for i in range(src.shape[0] // rows):
            at = pl.ds(i * rows, rows)
            wide[at, :] = src[at, :].astype(jnp.float32)
            copy = pltpu.make_async_copy(wide.at[at], dst.at[at], sems.at[len(copies)])
            copy.start()
            copies.append(copy)
    in_grad_out[...] = in_grad[...]
    taps_out[...] = taps[...]
    groups = rows_gate_out.shape[0] // LANES
    for i in range(groups):
        rows_gate_out[pl.ds(i * LANES, LANES)] = rows_gu[i]
        rows_up_out[pl.ds(i * LANES, LANES)] = rows_gu[groups + i]
    for i in range(rows_down_out.shape[0] // LANES):
        rows_down_out[pl.ds(i * LANES, LANES)] = rows_d[i]
    for copy in copies:
        copy.wait()


def fits(shape, inputs, w_gate):
    n_rep, n_fs, n_tp = shape["rep"], shape["fs"], shape["tp"]
    tok, feat = inputs.shape
    return (
        n_rep == 4 and n_fs == 4 and n_tp == 2 and feat == 2 * CW and 2 * CW <= w_gate.shape[1]
        and w_gate.shape[1] % CW == 0 and w_gate.shape[1] <= 1536 and tok % LANES == 0 and tok <= 512
    )


def fused_shards(shape, inputs, w_gate, w_up, conv_taps, w_down, out_grad):
    if not fits(shape, inputs, w_gate):
        return shards(inputs, w_gate, w_up, conv_taps, w_down, out_grad)
    n_rep, n_fs = shape["rep"], shape["fs"]
    tok, feat = inputs.shape
    hid = w_gate.shape[1]
    cw = CW
    chunks = hid // cw
    subs = feat // cw
    per = cw // LANES
    pieces = chunks * 3 * subs
    span = tok // 2 + HALO
    bf16, f32 = jnp.bfloat16, jnp.float32
    vmem = pl.BlockSpec(memory_space=pltpu.VMEM)
    hbm = pl.BlockSpec(memory_space=pltpu.HBM)
    hops = chunks * 3 * (n_fs - 1)
    dma = pltpu.SemaphoreType.DMA
    local = pltpu.VMEM
    whole = jax.ShapeDtypeStruct
    in_grad, down, gate, up, taps, rows_gu, rows_d = pl.pallas_call(
        functools.partial(layer_kernel, n_rep, n_fs),
        out_shape=(
            local((tok // 2, feat), bf16),
            local((hid, feat), bf16),
            local((feat, hid), bf16),
            local((feat, hid), bf16),
            local((KW, hid), f32),
            local((2 * subs * per, LANES), f32),
            local((chunks * per, LANES), f32),
        ),
        in_specs=[hbm, hbm, hbm, vmem, hbm, hbm],
        out_specs=(vmem,) * 7,
        scratch_shapes=[
            local((tok, feat), bf16),
            local((feat, hid), bf16),
            local((feat, hid), bf16),
            local((hid, feat), bf16),
            local((tok, feat), bf16),
            local((subs, cw, tok), bf16),
            local((chunks, 3, n_fs, span, LANES), bf16),
            local((chunks, 3, n_fs - 1, span, LANES), bf16),
            local((4, span, LANES), f32),
            local((chunks, cw, tok), bf16),
            local((chunks, tok, cw), bf16),
            local((chunks, tok, cw), bf16),
            local((RING, cw, cw), f32),
            local((pieces, cw, cw), bf16),
            local((pieces, cw, cw), bf16),
            local((pieces, cw, cw), bf16),
            local((pieces, cw, cw), bf16),
            local((tok, feat), f32),
            local((tok, feat), bf16),
            local((tok // 2, feat), bf16),
            local((n_fs, chunks * KW, LANES), f32),
            local((per, chunks * KW, LANES), f32),
            local((per, chunks * KW, LANES), f32),
            local((per, chunks * KW, LANES), f32),
            local((per, chunks * KW, LANES), f32),
            local((2 * subs * per, LANES), f32),
            local((chunks * per, LANES), f32),
            local((2 * subs * per, LANES), f32),
            local((n_fs - 1, chunks * per, LANES), f32),
            dma((hops,)), dma((hops,)), dma((chunks * 12,)), dma((chunks * 12,)),
            dma((pieces,)), dma((pieces,)), dma((pieces,)), dma((pieces,)), dma((8,)),
            dma((4 * (n_fs - 1) + 8,)),
        ],
        compiler_params=pltpu.CompilerParams(
            collective_id=0, has_side_effects=True, vmem_limit_bytes=50 * 1024 * 1024
        ),
    )(inputs, w_gate, w_up, conv_taps, w_down, out_grad)
    anywhere = pl.BlockSpec(memory_space=pl.ANY)
    copies = (2 * feat + hid) // cw
    gate, up, down, in_grad, taps, rows_gate, rows_up, rows_down = pl.pallas_call(
        finish_kernel,
        out_shape=(
            whole((feat, hid), f32), whole((feat, hid), f32), whole((hid, feat), f32),
            whole((tok // 2, feat), bf16), whole((KW, hid), f32),
            whole((feat,), f32), whole((feat,), f32), whole((hid,), f32),
        ),
        in_specs=[vmem] * 7,
        out_specs=(anywhere,) * 3 + (vmem,) * 5,
        scratch_shapes=[
            local((feat, hid), f32), local((feat, hid), f32), local((hid, feat), f32), dma((copies,)),
        ],
        compiler_params=pltpu.CompilerParams(vmem_limit_bytes=24 * 1024 * 1024),
    )(gate, up, down, in_grad, taps, rows_gu, rows_d)
    return (in_grad, gate, up, down, taps, rows_gate, rows_up, rows_down)


def solution(mesh):
    return jax.shard_map(
        functools.partial(fused_shards, dict(mesh.shape)),
        mesh=mesh,
        in_specs=(
            P("rep", "fs"),
            P("fs", "tp"),
            P("fs", "tp"),
            P(None, "tp"),
            P("tp", "fs"),
            P("rep", "fs"),
        ),
        out_specs=(
            P(("rep", "tp"), "fs"),
            P("fs", "tp"),
            P("fs", "tp"),
            P("tp", "fs"),
            P(None, "tp"),
            P("fs"),
            P("fs"),
            P("tp"),
        ),
        check_vma=False,
    )
```

time: 174 us -> 146 us (0.84)
  Pallas kernels: 162 us -> 145 us
  other arithmetic: 8.39 us -> 0 us
  local copies, waits for them, and re-layouts: 2.5 us -> 0 us
    pallas_call x1 -> x2, Pallas kernels: 162 us -> 145 us  [the longest x1 140 us: fused_shards(): pl.pallas_call(functools.partial(layer_kernel, n_rep, n_fs), out_shape=(l...]
    convert_element_type x3 -> x0, other arithmetic: 7.77 us -> none  [the longest x1 3.6 us: fused_shards(): up.astype(f32)]
    unnamed x18 -> x0, local copies, waits for them, and re-layouts: 2.5 us -> none
where the time goes in v1:
time: 146 us; the launch traced here: 145 us
  Pallas kernels  145 us (99%)
    pallas_call x1, Pallas kernels, fused_shards(): pl.pallas_call(functools.partial(layer_kernel, n_rep, n_fs), out_shape=(l...  140 us
    pallas_call x1, Pallas kernels, fused_shards(): pl.pallas_call(finish_kernel, out_shape=(whole((feat, hid), f32), whole((...  4.52 us

profile of v1, /device:TPU:0, one launch (start us, length us, event | category | flops | bytes accessed | tf_op | source)
XLA Modules:
  0.0 145.3 jit_solution(7979475024302250841)
XLA Ops:
  0.6 140.2 %shard_map.125 = (bf16[256,512]{1,0:T(8,128)(2,1)S(1)}, bf16[1536,512]{1,0:T(8,128)(2,1)S(1)}, bf16[512,1536]{1,0:T(8,128)(2,1)S(1)}, bf16[512,1536]{1,0:T(8,128...) custom-call(bf16[512,512]{1,0:T(8,128)(2,1)} %x_hbm.1, bf16[512,1536]{1,0:T(8,128)(2,1)} %wg_hbm.1, ...), custom_call_target="tpu_custom_call" | custom-call | tf_op jit(solution)/shard_map/pallas_call | solution.py:633
  140.8 4.5 %shard_map.126 = (f32[512,1536]{1,0:T(8,128)}, f32[512,1536]{1,0:T(8,128)}, f32[1536,512]{1,0:T(8,128)}, bf16[256,512]{1,0:T(8,128)(2,1)}, f32[3,1536]{1,0:T(4,1...) custom-call(bf16[512,1536]{1,0:T(8,128)(2,1)S(1)} %get-tuple-element.23.gate, ...), custom_call_target="tpu_custom_call" | custom-call | tf_op jit(solution)/shard_map/pallas_call | solution.py:686

commit v2 on v1

--- a/solution.py
+++ b/solution.py
@@ -96,30 +96,32 @@
 LANES = 128
 CW = 256
 HALO = 16
-A_LAG = 2
-B_LAG = 4
-OUT_LAG = 10
-RING = 4
+A_LAG = 0
+B_LAG = 3
+OUT_LAG = 18
+RING = 2
+WIDE = 4
+KEEP = 24
 MESH_ID = pl.DeviceIdType.MESH
 
 STEPS = (
+    (("grads", 0, 0), ("gather", 0, 1), ("reduce", 1, 0)),
+    (("reduce", 1, 1), ("gather", 0, 2)),
     (),
-    (("forward", 0, 1), ("reduce", 1, 1)),
-    (("forward", 0, 2),),
-    (("reduce", 1, 2),),
+    (("combine", 1, 0), ("combine", 1, 1), ("forward", 0, 2), ("reduce", 1, 2)),
     (("hidden", 1, 0),),
-    (("grads", 1, 0), ("forward", 1, 0), ("gather", 1, 1), ("gather", 1, 2), ("reduce", 2, 0)),
+    (("combine", 1, 2),),
 )
 
 
 def layer_kernel(
     n_rep, n_fs,
     x_hbm, wg_hbm, wu_hbm, taps_ref, wd_hbm, og_hbm,
-    in_grad_ref, down_ref, gate_ref, up_ref, taps_out_ref, rows_gu_ref, rows_down_ref,
+    in_grad_out, down_ref, gate_ref, up_ref, taps_out, rows_gu_out, rows_down_out,
     x_ref, wg_ref, wu_ref, wd_ref, og_ref,
-    xt, send_part, recv_part, held, h_all, g_all, u_all, ring, part, from_out, from_in, tot,
-    acc, ig_send, ig_recv, tap_all, tap_two, tap_out, tap_in, tap_sum, rows_gu, rows_d, rows_tp, rows_fs,
-    rs_send, rs_recv, ag_send, ag_recv, a_send, out_recv, in_recv, b_send, loc_sem, misc,
+    xt, send_part, recv_part, pair_part, held, h_all, g_all, u_all, ring, wide, part, from_out, from_in, tot,
+    acc, ig_send, ig_recv, in_grad_ref, taps_out_ref, rows_gu_ref, rows_down_ref, tap_all, tap_two, tap_out, tap_in, tap_sum, rows_gu, rows_d, rows_tp, rows_fs,
+    rs_send, rs_recv, ag_send, ag_recv, a_send, out_recv, in_recv, b_send, wide_sem, out_sem, loc_sem, misc,
 ):
     tok, feat = x_ref.shape
     cw = CW
@@ -189,11 +191,23 @@
             return slice(c * cw, (c + 1) * cw)
         return pl.ds(pl.multiple_of(c * cw, cw), cw)
 
-    def rs_copy(c, tensor, k):
-        s = (c * 3 + tensor) * (n_fs - 1) + k
+    cut = recv_part.shape[3]
+    halves = (slice(0, cut), slice(cut, span))
+
+    def rs_copy(c, tensor, n):
+        s = (lax.rem(c, 2) * 3 + tensor) * 6 + n
+        side_of = n % 2
+        near, far = (beside, across) if side_of == 0 else (across, beside)
+        rows = halves[side_of]
+        size = rows.stop - rows.start
+        owner = corner if n < 2 else near
+        target = near if n < 4 else far
+        if n < 4:
+            src = send_part.at[c, tensor, owner, rows]
+        else:
+            src = pair_part.at[c, tensor, side_of, 0:size]
         return remote(
-            send_part.at[c, tensor, peers[k]], recv_part.at[c, tensor, k],
-            rs_send.at[s], rs_recv.at[s], {"fs": peers[k]},
+            src, recv_part.at[c, tensor, n, 0:size], rs_send.at[n], rs_recv.at[s], {"fs": target}
         )
 
     def product(c, tensor):
@@ -211,19 +225,34 @@
             send_part[c, tensor, g] = value[row : row + span, lane : lane + LANES]
 
     def reduce_send(c, tensor):
-        for k in range(n_fs - 1):
-            rs_copy(c, tensor, k).start()
+        for n in range(4):
+            rs_copy(c, tensor, n).start()
 
     def reduce_start(c, tensor):
         product(c, tensor)
         reduce_send(c, tensor)
 
+    def combine(c, tensor):
+        for n in range(2):
+            rows = halves[n]
+            size = rows.stop - rows.start
+            rs_copy(c, tensor, n).wait_recv()
+            mine = send_part[c, tensor, across if n == 0 else beside, rows]
+            pair_part[c, tensor, n, 0:size] = (
+                mine.astype(f32) + recv_part[c, tensor, n, 0:size].astype(f32)
+            ).astype(bf16)
+            rs_copy(c, tensor, 4 + n).start()
+
     def reduced(c, tensor):
-        value = send_part[c, tensor, f].astype(f32)
-        for k in range(n_fs - 1):
-            rs_copy(c, tensor, k).wait_recv()
-            value = value + recv_part[c, tensor, k].astype(f32)
-        return value.astype(bf16).astype(f32)
+        parts = []
+        for n in range(2):
+            rows = halves[n]
+            size = rows.stop - rows.start
+            rs_copy(c, tensor, 2 + n).wait_recv()
+            value = send_part[c, tensor, f, rows].astype(f32) + recv_part[c, tensor, 2 + n, 0:size].astype(f32)
+            rs_copy(c, tensor, 4 + n).wait_recv()
+            parts.append(value + recv_part[c, tensor, 4 + n, 0:size].astype(f32))
+        return jnp.concatenate(parts, axis=0).astype(bf16).astype(f32)
 
     def block(c, tensor, owner, part_of=None):
         col = lax.rem(owner, 2) * LANES
@@ -240,7 +269,7 @@
         return ref.at[c, pl.ds(pl.multiple_of(start, size), size), pl.ds(pl.multiple_of(col, LANES), LANES)]
 
     def ag_copy(c, tensor, step, owner):
-        s = (c * 3 + tensor) * 4
+        s = (lax.rem(c, 2) * 3 + tensor) * 4
         if step == 0:
             ref, slot, target = block(c, tensor, owner), 0, beside
         elif step == 1:
@@ -249,11 +278,17 @@
             ref, slot, target = block(c, tensor, owner, 1), 2, beside
         else:
             ref, slot, target = block(c, tensor, owner, 0), 3, across
-        return remote(ref, ref, ag_send.at[s + slot], ag_recv.at[s + slot], {"fs": target})
+        return remote(ref, ref, ag_send.at[slot], ag_recv.at[s + slot], {"fs": target})
+
+    def corner_copy(c, tensor, owner):
+        ref, s = block(c, tensor, owner), (lax.rem(c, 2) * 3 + tensor) * 4 + 2
+        return remote(ref, ref, ag_send.at[2], ag_recv.at[s], {"fs": corner})
 
     def gather_start(c, tensor):
         for step in (0, 1):
             ag_copy(c, tensor, step, f).start()
+        if tensor < 2:
+            corner_copy(c, tensor, f).start()
 
     def forward(c, tensor):
         ag_copy(c, tensor, 0, beside).wait_recv()
@@ -262,8 +297,13 @@
         ag_copy(c, tensor, 2, across).start()
 
     def gathered(c, tensor):
-        ag_copy(c, tensor, 2, corner).wait_recv()
-        ag_copy(c, tensor, 3, corner).wait_recv()
+        if tensor < 2:
+            ag_copy(c, tensor, 0, beside).wait_recv()
+            ag_copy(c, tensor, 1, across).wait_recv()
+            corner_copy(c, tensor, corner).wait_recv()
+        else:
+            ag_copy(c, tensor, 2, corner).wait_recv()
+            ag_copy(c, tensor, 3, corner).wait_recv()
 
     def own(value):
         return jnp.where(top == 0, value[:own_rows], value[HALO:])
@@ -314,58 +354,89 @@
                 own(down(gate, KW - 1 - j) * pre_grad), axis=0, keepdims=True
             )
 
-    def part_copy(p):
-        return remote(part.at[p], from_out.at[p], a_send.at[p], out_recv.at[p], {"rep": toward})
-
-    def exchange_copy(p):
-        return remote(part.at[p], from_in.at[p], a_send.at[p], in_recv.at[p], {"rep": toward})
-
-    def total_copy(p, src):
-        return remote(src.at[p], from_in.at[p], b_send.at[p], in_recv.at[p], {"rep": outward})
-
-    def finished(c, s, value):
+    def half_rows(h):
+        return slice(h * LANES, (h + 1) * LANES)
+
+    def part_copy(p, h):
+        rows = half_rows(h)
+        s = lax.rem(p * per + h, KEEP)
+        return remote(part.at[p, rows], from_out.at[p, rows], a_send.at[0], out_recv.at[s], {"rep": toward})
+
+    def exchange_copy(p, h):
+        rows = half_rows(h)
+        s = lax.rem(p * per + h, KEEP)
+        return remote(part.at[p, rows], from_in.at[p, rows], a_send.at[0], in_recv.at[s], {"rep": toward})
+
+    def total_copy(p, h):
+        rows = half_rows(h)
+        s = lax.rem(p * per + h, KEEP)
+        return remote(tot.at[p, rows], from_in.at[p, rows], b_send.at[0], in_recv.at[s], {"rep": outward})
+
+    def piece_rows(base, h):
+        if isinstance(base, int):
+            return slice(base + h * LANES, base + (h + 1) * LANES)
+        return pl.ds(pl.multiple_of(base + h * LANES, LANES), LANES)
+
+    def place(c, s, h):
         tensor, q = s // subs, s % subs
-        inner = slice(q * cw, (q + 1) * cw)
+        slot = (s * per + h) % WIDE
         if tensor == 0:
-            down_ref[chunk_cols(c), inner] = value
+            dst = down_ref.at[piece_rows(c * cw, h), q * cw : (q + 1) * cw]
         elif tensor == 1:
-            gate_ref[inner, chunk_cols(c)] = value
-        else:
-            up_ref[inner, chunk_cols(c)] = value
+            dst = gate_ref.at[piece_rows(q * cw, h), chunk_cols(c)]
+        else:
+            dst = up_ref.at[piece_rows(q * cw, h), chunk_cols(c)]
+        return pltpu.make_async_copy(wide.at[slot], dst, wide_sem.at[slot])
+
+    def finished(c, s, h, value):
+        tensor, q = s // subs, s % subs
         value = value.astype(f32)
+        slot = (s * per + h) % WIDE
+        copy = place(c, s, h)
+        if not isinstance(c, int):
+            pl.when((c * slots + s) * per + h >= WIDE)(copy.wait)
+        elif (c * slots + s) * per + h >= WIDE:
+            copy.wait()
+        wide[slot] = value
+        copy.start()
         square = value * value
         lanes = square[:, :LANES]
         for g in range(1, cw // LANES):
             lanes = lanes + square[:, g * LANES : (g + 1) * LANES]
-        for i in range(per):
-            row = jnp.sum(lanes[i * LANES : (i + 1) * LANES].T, axis=0, keepdims=True)
-            if tensor == 0:
-                at = pl.ds(c * per + i, 1)
-                rows_d[at, :] = row if q == 0 else rows_d[at, :] + row
-            else:
-                at = ((tensor - 1) * subs + q) * per + i
-                rows_gu[at : at + 1, :] = rows_gu[at : at + 1, :] + row
-
-    def stage_a(p):
-        part_copy(p).wait_recv()
-        part[p] = (ring[lax.rem(p, RING)] + from_out[p].astype(f32)).astype(bf16)
-        exchange_copy(p).start()
-
-    def stage_b(c, s):
+        row = jnp.sum(lanes.T, axis=0, keepdims=True)
+        if tensor == 0:
+            at = pl.ds(c * per + h, 1)
+            rows_d[at, :] = row if q == 0 else rows_d[at, :] + row
+        else:
+            at = ((tensor - 1) * subs + q) * per + h
+            rows_gu[at : at + 1, :] = rows_gu[at : at + 1, :] + row
+
+    def stage_a(p, h):
+        part_copy(p, h).wait_recv()
+        rows = half_rows(h)
+        part[p, rows] = (ring[lax.rem(p, RING), rows] + from_out[p, rows].astype(f32)).astype(bf16)
+        exchange_copy(p, h).start()
+
+    def stage_b(c, s, h):
         p = c * slots + s
-        exchange_copy(p).wait_recv()
-        value = (part[p].astype(f32) + from_in[p].astype(f32)).astype(bf16)
-        tot[p] = value
-        total_copy(p, tot).start()
-        finished(c, s, value)
-
-    def stage_out(c, s):
-        exchange_copy(c * slots + s).wait_recv()
-        finished(c, s, from_in[c * slots + s])
-
-    def behind(c, s, lag):
-        back = (lag - s + slots - 1) // slots if lag > s else 0
-        return c - back, s - lag + back * slots, back
+        rows = half_rows(h)
+        exchange_copy(p, h).wait_recv()
+        value = (part[p, rows].astype(f32) + from_in[p, rows].astype(f32)).astype(bf16)
+        tot[p, rows] = value
+        total_copy(p, h).start()
+        finished(c, s, h, value)
+
+    def stage_out(c, s, h):
+        p = c * slots + s
+        exchange_copy(p, h).wait_recv()
+        finished(c, s, h, from_in[p, half_rows(h)])
+
+    def behind(c, s, h, lag):
+        steps = slots * per
+        at = s * per + h - lag
+        back = (-at + steps - 1) // steps if at < 0 else 0
+        at += back * steps
+        return c - back, at // per, at % per, back
 
     def guarded(c, lowest, fn):
         if isinstance(c, int):
@@ -387,21 +458,24 @@
             value = jnp.dot(xt[q], g_all[c], preferred_element_type=f32)
         else:
             value = jnp.dot(xt[q], u_all[c], preferred_element_type=f32)
-        ca, sa, ka = behind(c, s, A_LAG)
-        cb, sb, kb = behind(c, s, B_LAG)
-        co, so, ko = behind(c, s, OUT_LAG)
 
         @pl.when(is_end)
         def _():
-            part[p] = value.astype(bf16)
-            part_copy(p).start()
-            guarded(c, ko, lambda: stage_out(co, so))
+            for h in range(per):
+                part[p, half_rows(h)] = value[half_rows(h)].astype(bf16)
+                part_copy(p, h).start()
+            for h in range(per):
+                co, so, ho, ko = behind(c, s, h, OUT_LAG)
+                guarded(c, ko, functools.partial(stage_out, co, so, ho))
 
         @pl.when(is_mid)
         def _():
             ring[lax.rem(p, RING)] = value
-            guarded(c, ka, lambda: stage_a(ca * slots + sa))
-            guarded(c, kb, lambda: stage_b(cb, sb))
+            for h in range(per):
+                ca, sa, ha, ka = behind(c, s, h, A_LAG)
+                guarded(c, ka, functools.partial(stage_a, ca * slots + sa, ha))
+                cb, sb, hb, kb = behind(c, s, h, B_LAG)
+                guarded(c, kb, functools.partial(stage_b, cb, sb, hb))
 
     def input_term(c):
         cols = chunk_cols(c)
@@ -414,6 +488,7 @@
     actions = {
         "forward": forward,
         "reduce": reduce_start,
+        "combine": combine,
         "hidden": lambda c, tensor: hidden_step(c),
         "grads": lambda c, tensor: grads_step(c),
         "gather": gather_start,
@@ -430,10 +505,75 @@
         else:
             pl.when(target < chunks)(lambda: actions[name](target, tensor))
 
-    def body(c):
+    m = 2 * (n_fs - 1)
+    half = tok // 2
+    ig_copy = remote(
+        ig_send.at[pl.ds(pl.multiple_of((1 - t) * half, half), half)], ig_recv,
+        misc.at[m], misc.at[m + 1], {"tp": 1 - t},
+    )
+    tap_peers = [
+        remote(tap_all.at[f], tap_all.at[f], misc.at[2 * k], misc.at[2 * k + 1], {"fs": peers[k]})
+        for k in range(n_fs - 1)
+    ]
+    tap_part = remote(tap_two, tap_out, misc.at[m + 2], misc.at[m + 3], {"rep": toward})
+    tap_exchange = remote(tap_two, tap_in, misc.at[m + 2], misc.at[m + 4], {"rep": toward})
+    tap_total = remote(tap_sum, tap_in, misc.at[m + 5], misc.at[m + 4], {"rep": outward})
+    fs_rows = [
+        remote(rows_d, rows_fs.at[k], misc.at[m + 8 + 2 * k], misc.at[m + 9 + 2 * k], {"fs": peers[k]})
+        for k in range(n_fs - 1)
+    ]
+    tp_rows = remote(rows_gu, rows_tp, misc.at[m + 6], misc.at[m + 7], {"tp": 1 - t})
+
+    outputs = [
+        pltpu.make_async_copy(src, dst, out_sem.at[n])
+        for n, (src, dst) in enumerate((
+            (in_grad_ref, in_grad_out), (taps_out_ref, taps_out),
+            (rows_down_ref, rows_down_out), (rows_gu_ref, rows_gu_out),
+        ))
+    ]
+
+    def tap_first():
+        for copy in tap_peers:
+            copy.wait()
+        for i in range(per):
+            tap_two[i] = tap_all[i] + tap_all[i + 2]
+        pl.when(is_end)(tap_part.start)
+
+    def tap_second():
+        tap_part.wait_recv()
+        tap_two[...] = tap_two[...] + tap_out[...]
+        tap_exchange.start()
+
+    def tap_place():
+        for c in range(chunks):
+            for i in range(per):
+                lane = (c * per + i) * LANES
+                taps_out_ref[:, lane : lane + LANES] = tap_sum[i, c * KW : (c + 1) * KW, :]
+        outputs[1].start()
+
+    def input_start():
+        ig_send[...] = acc[...].astype(bf16)
+        ig_copy.start()
+
+    def input_finish():
+        ig_copy.wait()
+        in_grad_ref[...] = (
+            ig_send[pl.ds(pl.multiple_of(t * half, half), half), :].astype(f32) + ig_recv[...].astype(f32)
+        ).astype(bf16)
+        outputs[0].start()
+
+    def body(c, last=False):
         for s in range(slots):
-            for step in STEPS[s]:
-                run(step, c)
+            if s > 0 or not isinstance(c, int) or c > 0:
+                for step in STEPS[s]:
+                    run(step, c)
+            if last and s == 1:
+                for copy in tap_peers:
+                    copy.start()
+            if last and s == 3:
+                tap_first()
+            if last and s == slots - 2:
+                pl.when(is_mid)(tap_second)
             work(c, s)
         input_term(c)
 
@@ -447,129 +587,95 @@
     reduce_send(0, 1)
     loads[3].wait()
     loads[4].wait()
-    reduce_start(0, 2)
+    product(0, 2)
     for q in range(subs):
         xt[q] = x_ref[:, q * cw : (q + 1) * cw].astype(f32).T.astype(bf16)
     rows_gu[...] = jnp.zeros_like(rows_gu)
     for copy in loads[5:]:
         copy.wait()
+    combine(0, 0)
+    combine(0, 1)
+    reduce_send(0, 2)
+    if chunks > 1:
+        product(1, 0)
     hidden_step(0)
+    combine(0, 2)
     grads_step(0)
-    forward(0, 0)
     gather_start(0, 1)
-    gather_start(0, 2)
     if chunks > 1:
-        reduce_start(1, 0)
+        reduce_send(1, 0)
     body(0)
 
-    @pl.loop(1, chunks)
+    @pl.loop(1, chunks - 1)
     def _(c):
         body(c)
 
-    m = 2 * (n_fs - 1)
-    half = tok // 2
-    ig_send[...] = acc[...].astype(bf16)
-    ig_copy = remote(
-        ig_send.at[pl.ds(pl.multiple_of((1 - t) * half, half), half)], ig_recv,
-        misc.at[m], misc.at[m + 1], {"tp": 1 - t},
-    )
-    ig_copy.start()
-
-    tap_peers = []
-    for k in range(n_fs - 1):
-        tap_peers.append(remote(
-            tap_all.at[f], tap_all.at[f], misc.at[2 * k], misc.at[2 * k + 1], {"fs": peers[k]}
-        ))
-        tap_peers[k].start()
-    tap_part = remote(tap_two, tap_out, misc.at[m + 2], misc.at[m + 3], {"rep": toward})
-    tap_exchange = remote(tap_two, tap_in, misc.at[m + 2], misc.at[m + 4], {"rep": toward})
-    tap_total = remote(tap_sum, tap_in, misc.at[m + 5], misc.at[m + 4], {"rep": outward})
-
-    def tap_first():
-        for copy in tap_peers:
-            copy.wait()
-        for i in range(per):
-            tap_two[i] = tap_all[i] + tap_all[i + 2]
-
-    def input_finish():
-        ig_copy.wait()
-        in_grad_ref[...] = (
-            ig_send[pl.ds(pl.multiple_of(t * half, half), half), :].astype(f32) + ig_recv[...].astype(f32)
-        ).astype(bf16)
-
-    fs_rows = [
-        remote(rows_d, rows_fs.at[k], misc.at[m + 8 + 2 * k], misc.at[m + 9 + 2 * k], {"fs": peers[k]})
-        for k in range(n_fs - 1)
-    ]
-    tp_rows = remote(rows_gu, rows_tp, misc.at[m + 6], misc.at[m + 7], {"tp": 1 - t})
-
-    def rows_done(p, lag):
-        if p == total_pieces - min(lag, slots - subs + 1):
-            for copy in fs_rows:
-                copy.start()
-        if p == total_pieces - 1:
-            tp_rows.start()
+    body(chunks - 1, last=True)
+    input_start()
+    down_last = total_pieces - slots + subs - 1
+
+    steps = total_pieces * per
 
     @pl.when(is_end)
     def _():
-        tap_first()
-        tap_part.start()
-        input_finish()
-        for p in range(total_pieces - OUT_LAG, total_pieces):
-            stage_out(p // slots, p % slots)
-            rows_done(p, OUT_LAG)
-        tap_exchange.wait_recv()
-        tap_sum[...] = tap_in[...]
+        for k in range(steps - OUT_LAG, steps):
+            p = k // per
+            if k == steps - 1:
+                input_finish()
+                tap_exchange.wait_recv()
+                tap_sum[...] = tap_in[...]
+                tap_place()
+            stage_out(p // slots, p % slots, k % per)
+            if k == max(steps - OUT_LAG, (down_last + 1) * per - 1):
+                for copy in fs_rows:
+                    copy.start()
 
     @pl.when(is_mid)
     def _():
-        for s in range(total_pieces, total_pieces + B_LAG):
-            if s - A_LAG < total_pieces:
-                stage_a(s - A_LAG)
-            if s == total_pieces:
-                tap_first()
-            if s == total_pieces + A_LAG:
-                tap_part.wait_recv()
-                tap_two[...] = tap_two[...] + tap_out[...]
-                tap_exchange.start()
+        for copy in fs_rows:
+            copy.start()
+        for k in range(steps, steps + B_LAG):
+            if k - A_LAG < steps:
+                stage_a((k - A_LAG) // per, (k - A_LAG) % per)
+            p = (k - B_LAG) // per
+            stage_b(p // slots, p % slots, (k - B_LAG) % per)
+            if k == steps:
+                tap_exchange.wait_recv()
+                tap_sum[...] = tap_two[...] + tap_in[...]
+                tap_total.start()
                 input_finish()
-            stage_b((s - B_LAG) // slots, (s - B_LAG) % slots)
-            rows_done(s - B_LAG, B_LAG)
-        tap_exchange.wait_recv()
-        tap_sum[...] = tap_two[...] + tap_in[...]
-        tap_total.start()
-
-    for c in range(chunks):
-        for i in range(per):
-            lane = (c * per + i) * LANES
-            taps_out_ref[:, lane : lane + LANES] = tap_sum[i, c * KW : (c + 1) * KW, :]
-
-    @pl.loop(0, chunks * 3)
-    def _(n):
-        c, tensor = n // 3, lax.rem(n, 3)
-        for k in range(n_fs - 1):
-            rs_copy(c, tensor, k).wait_send()
-        for step, owner in ((0, f), (1, f), (2, across), (3, beside)):
-            s = n * 4
-            size = own_rows if step < 2 else own_rows // 2
-            ref = g_all.at[c, pl.ds(0, size), pl.ds(0, LANES)]
-            remote(ref, ref, ag_send.at[s + step], ag_recv.at[s + step], {"fs": beside}).wait_send()
-
+                tap_place()
+
+    tp_rows.start()
+
+    def all_sent(ref, sem):
+        remote(ref, ref, sem, sem, {"tp": 1 - t}).wait_send()
+
+    for n in range(6):
+        rows = halves[n % 2]
+        all_sent(recv_part.at[:, :, n, 0 : rows.stop - rows.start], rs_send.at[n])
+    columns = h_all.shape[1]
+    for slot, quarters in ((0, 12), (1, 12), (2, 10), (3, 2)):
+        all_sent(h_all.at[:, 0 : columns * quarters // 16], ag_send.at[slot])
+    all_sent(part, a_send.at[0])
     tap_part.wait_send()
 
-    @pl.loop(0, total_pieces)
-    def _(p):
-        part_copy(p).wait_send()
-
-        @pl.when(is_mid)
-        def _():
-            total_copy(p, tot).wait_send()
-
+    @pl.when(is_mid)
+    def _():
+        all_sent(tot, b_send.at[0])
+
+    for k in range(steps - WIDE, steps):
+        p = k // per
+        place(p // slots, p % slots, k % per).wait()
     for copy in fs_rows:
         copy.wait()
     rows_down_ref[...] = rows_d[...] + (rows_fs[0] + rows_fs[1] + rows_fs[2])
+    outputs[2].start()
     tp_rows.wait()
     rows_gu_ref[...] = rows_gu[...] + rows_tp[...]
+    outputs[3].start()
+    for copy in outputs:
+        copy.wait()
 
     @pl.when(is_mid)
     def _():
@@ -579,17 +685,13 @@
 def finish_kernel(
     gate, up, down, in_grad, taps, rows_gu, rows_d,
     gate_out, up_out, down_out, in_grad_out, taps_out, rows_gate_out, rows_up_out, rows_down_out,
-    wide_gate, wide_up, wide_down, sems,
+    sems,
 ):
-    rows = CW
     copies = []
-    for src, wide, dst in ((gate, wide_gate, gate_out), (up, wide_up, up_out), (down, wide_down, down_out)):
-        for i in range(src.shape[0] // rows):
-            at = pl.ds(i * rows, rows)
-            wide[at, :] = src[at, :].astype(jnp.float32)
-            copy = pltpu.make_async_copy(wide.at[at], dst.at[at], sems.at[len(copies)])
-            copy.start()
-            copies.append(copy)
+    for src, dst in ((gate, gate_out), (up, up_out), (down, down_out)):
+        copy = pltpu.make_async_copy(src, dst, sems.at[len(copies)])
+        copy.start()
+        copies.append(copy)
     in_grad_out[...] = in_grad[...]
     taps_out[...] = taps[...]
     groups = rows_gate_out.shape[0] // LANES
@@ -606,8 +708,8 @@
     n_rep, n_fs, n_tp = shape["rep"], shape["fs"], shape["tp"]
     tok, feat = inputs.shape
     return (
-        n_rep == 4 and n_fs == 4 and n_tp == 2 and feat == 2 * CW and 2 * CW <= w_gate.shape[1]
-        and w_gate.shape[1] % CW == 0 and w_gate.shape[1] <= 1536 and tok % LANES == 0 and tok <= 512
+        n_rep == 4 and n_fs == 4 and n_tp == 2 and feat == 2 * CW and 3 * CW <= w_gate.shape[1]
+        and w_gate.shape[1] % CW == 0 and w_gate.shape[1] <= 1536 and tok % (2 * LANES) == 0 and tok <= 512
     )
 
 
@@ -623,10 +725,11 @@
     per = cw // LANES
     pieces = chunks * 3 * subs
     span = tok // 2 + HALO
+    cut = -(-span // (2 * HALO)) * HALO
     bf16, f32 = jnp.bfloat16, jnp.float32
     vmem = pl.BlockSpec(memory_space=pltpu.VMEM)
     hbm = pl.BlockSpec(memory_space=pltpu.HBM)
-    hops = chunks * 3 * (n_fs - 1)
+    anywhere = pl.BlockSpec(memory_space=pl.ANY)
     dma = pltpu.SemaphoreType.DMA
     local = pltpu.VMEM
     whole = jax.ShapeDtypeStruct
@@ -634,15 +737,15 @@
         functools.partial(layer_kernel, n_rep, n_fs),
         out_shape=(
             local((tok // 2, feat), bf16),
-            local((hid, feat), bf16),
-            local((feat, hid), bf16),
-            local((feat, hid), bf16),
+            local((hid, feat), f32),
+            local((feat, hid), f32),
+            local((feat, hid), f32),
             local((KW, hid), f32),
             local((2 * subs * per, LANES), f32),
             local((chunks * per, LANES), f32),
         ),
         in_specs=[hbm, hbm, hbm, vmem, hbm, hbm],
-        out_specs=(vmem,) * 7,
+        out_specs=(anywhere,) * 7,
         scratch_shapes=[
             local((tok, feat), bf16),
             local((feat, hid), bf16),
@@ -651,12 +754,14 @@
             local((tok, feat), bf16),
             local((subs, cw, tok), bf16),
             local((chunks, 3, n_fs, span, LANES), bf16),
-            local((chunks, 3, n_fs - 1, span, LANES), bf16),
+            local((chunks, 3, 6, cut, LANES), bf16),
+            local((chunks, 3, 2, cut, LANES), bf16),
             local((4, span, LANES), f32),
             local((chunks, cw, tok), bf16),
             local((chunks, tok, cw), bf16),
             local((chunks, tok, cw), bf16),
             local((RING, cw, cw), f32),
+            local((WIDE, LANES, cw), f32),
             local((pieces, cw, cw), bf16),
             local((pieces, cw, cw), bf16),
             local((pieces, cw, cw), bf16),
@@ -664,6 +769,10 @@
             local((tok, feat), f32),
             local((tok, feat), bf16),
             local((tok // 2, feat), bf16),
+            local((tok // 2, feat), bf16),
+            local((KW, hid), f32),
+            local((2 * subs * per, LANES), f32),
+            local((chunks * per, LANES), f32),
             local((n_fs, chunks * KW, LANES), f32),
             local((per, chunks * KW, LANES), f32),
             local((per, chunks * KW, LANES), f32),
@@ -673,16 +782,14 @@
             local((chunks * per, LANES), f32),
             local((2 * subs * per, LANES), f32),
             local((n_fs - 1, chunks * per, LANES), f32),
-            dma((hops,)), dma((hops,)), dma((chunks * 12,)), dma((chunks * 12,)),
-            dma((pieces,)), dma((pieces,)), dma((pieces,)), dma((pieces,)), dma((8,)),
+            dma((6,)), dma((36,)), dma((4,)), dma((24,)),
+            dma((1,)), dma((KEEP,)), dma((KEEP,)), dma((1,)), dma((WIDE,)), dma((4,)), dma((8,)),
             dma((4 * (n_fs - 1) + 8,)),
         ],
         compiler_params=pltpu.CompilerParams(
             collective_id=0, has_side_effects=True, vmem_limit_bytes=50 * 1024 * 1024
         ),
     )(inputs, w_gate, w_up, conv_taps, w_down, out_grad)
-    anywhere = pl.BlockSpec(memory_space=pl.ANY)
-    copies = (2 * feat + hid) // cw
     gate, up, down, in_grad, taps, rows_gate, rows_up, rows_down = pl.pallas_call(
         finish_kernel,
         out_shape=(
@@ -690,11 +797,9 @@
             whole((tok // 2, feat), bf16), whole((KW, hid), f32),
             whole((feat,), f32), whole((feat,), f32), whole((hid,), f32),
         ),
-        in_specs=[vmem] * 7,
+        in_specs=[anywhere] * 3 + [vmem] * 4,
         out_specs=(anywhere,) * 3 + (vmem,) * 5,
-        scratch_shapes=[
-            local((feat, hid), f32), local((feat, hid), f32), local((hid, feat), f32), dma((copies,)),
-        ],
+        scratch_shapes=[dma((3,))],
         compiler_params=pltpu.CompilerParams(vmem_limit_bytes=24 * 1024 * 1024),
     )(gate, up, down, in_grad, taps, rows_gu, rows_d)
     return (in_grad, gate, up, down, taps, rows_gate, rows_up, rows_down)

time: 146 us -> 142 us (0.973)
  Pallas kernels: 145 us -> 141 us
    pallas_call x1, Pallas kernels: 140 us -> 136 us  [fused_shards(): pl.pallas_call(functools.partial(layer_kernel, n_rep, n_fs), out_shape=(l...]
where the time goes in v2:
time: 142 us
  Pallas kernels  141 us (99%)
    pallas_call x1, Pallas kernels, fused_shards(): pl.pallas_call(functools.partial(layer_kernel, n_rep, n_fs), out_shape=(l...  136 us
    pallas_call x1, Pallas kernels, fused_shards(): pl.pallas_call(finish_kernel, out_shape=(whole((feat, hid), f32), whole((...  4.48 us

profile of v2, /device:TPU:0, one launch (start us, length us, event | category | flops | bytes accessed | tf_op | source)
XLA Modules:
  0.0 141.6 jit_solution(15896825041570218687)
XLA Ops:
  0.6 136.3 %shard_map.125 = (bf16[256,512]{1,0:T(8,128)(2,1)S(1)}, f32[1536,512]{1,0:T(8,128)S(1)}, f32[512,1536]{1,0:T(8,128)S(1)}, f32[512,1536]{1,0:T(8,128)S(1)}, f32[3...) custom-call(bf16[512,512]{1,0:T(8,128)(2,1)} %x_hbm.1, bf16[512,1536]{1,0:T(8,128)(2,1)} %wg_hbm.1, ...), custom_call_target="tpu_custom_call" | custom-call | tf_op jit(solution)/shard_map/pallas_call | solution.py:736
  136.9 4.5 %shard_map.126 = (f32[512,1536]{1,0:T(8,128)}, f32[512,1536]{1,0:T(8,128)}, f32[1536,512]{1,0:T(8,128)}, bf16[256,512]{1,0:T(8,128)(2,1)}, f32[3,1536]{1,0:T(4,1...) custom-call(f32[512,1536]{1,0:T(8,128)S(1)} %get-tuple-element.23.gate, f32[512,1536]{1,0:T(8,128)S(1)} %get-tuple-element.24.up, ...), custom_call_target="tpu_custom_call" | custom-call | tf_op jit(solution)/shard_map/pallas_call | solution.py:793

commit v3 on v2

--- a/solution.py
+++ b/solution.py
@@ -96,8 +96,8 @@
 LANES = 128
 CW = 256
 HALO = 16
-A_LAG = 0
-B_LAG = 3
+A_LAG = 1
+B_LAG = 4
 OUT_LAG = 18
 RING = 2
 WIDE = 4
@@ -106,12 +106,13 @@
 
 STEPS = (
     (("grads", 0, 0), ("gather", 0, 1), ("reduce", 1, 0)),
-    (("reduce", 1, 1), ("gather", 0, 2)),
-    (),
-    (("combine", 1, 0), ("combine", 1, 1), ("forward", 0, 2), ("reduce", 1, 2)),
-    (("hidden", 1, 0),),
-    (("combine", 1, 2),),
+    (("forward", 0, 1), ("gather", 0, 2)),
+    (("combine", 1, 0), ("combine", 1, 1), ("reduce", 1, 2)),
+    (("forward", 0, 2),),
+    (("hidden", 1, 0), ("combine", 1, 2), ("reduce", 2, 1)),
+    (("forward", 1, 0),),
 )
+FIRST_STEPS = ((), (("gather", 0, 2),), (), STEPS[2] + STEPS[3]) + STEPS[4:]
 
 
 def layer_kernel(
@@ -121,7 +122,7 @@
     x_ref, wg_ref, wu_ref, wd_ref, og_ref,
     xt, send_part, recv_part, pair_part, held, h_all, g_all, u_all, ring, wide, part, from_out, from_in, tot,
     acc, ig_send, ig_recv, in_grad_ref, taps_out_ref, rows_gu_ref, rows_down_ref, tap_all, tap_two, tap_out, tap_in, tap_sum, rows_gu, rows_d, rows_tp, rows_fs,
-    rs_send, rs_recv, ag_send, ag_recv, a_send, out_recv, in_recv, b_send, wide_sem, out_sem, loc_sem, misc,
+    rs_send, rs_recv, ag_send, ag_recv, a_send, out_recv, in_recv, b_send, wide_sem, out_sem, loc_sem, go_sem, misc,
 ):
     tok, feat = x_ref.shape
     cw = CW
@@ -280,14 +281,17 @@
             ref, slot, target = block(c, tensor, owner, 0), 3, across
         return remote(ref, ref, ag_send.at[slot], ag_recv.at[s + slot], {"fs": target})
 
+    def direct(c, tensor):
+        return isinstance(c, int) and c == 0 and tensor < 2
+
     def corner_copy(c, tensor, owner):
-        ref, s = block(c, tensor, owner), (lax.rem(c, 2) * 3 + tensor) * 4 + 2
-        return remote(ref, ref, ag_send.at[2], ag_recv.at[s], {"fs": corner})
+        ref = block(c, tensor, owner)
+        return remote(ref, ref, ag_send.at[4], ag_recv.at[tensor * 4 + 2], {"fs": corner})
 
     def gather_start(c, tensor):
         for step in (0, 1):
             ag_copy(c, tensor, step, f).start()
-        if tensor < 2:
+        if direct(c, tensor):
             corner_copy(c, tensor, f).start()
 
     def forward(c, tensor):
@@ -296,14 +300,19 @@
         ag_copy(c, tensor, 1, across).wait_recv()
         ag_copy(c, tensor, 2, across).start()
 
-    def gathered(c, tensor):
-        if tensor < 2:
-            ag_copy(c, tensor, 0, beside).wait_recv()
-            ag_copy(c, tensor, 1, across).wait_recv()
-            corner_copy(c, tensor, corner).wait_recv()
-        else:
+    def gathered(c, tensor, q):
+        if direct(c, tensor):
+            if q == 0:
+                ag_copy(c, tensor, 1, across).wait_recv()
+            if q == tensor ^ 1:
+                ag_copy(c, tensor, 0, beside).wait_recv()
+                corner_copy(c, tensor, corner).wait_recv()
+        elif q == (1 if tensor == 0 else 0):
             ag_copy(c, tensor, 2, corner).wait_recv()
             ag_copy(c, tensor, 3, corner).wait_recv()
+
+    def hidden_side(q):
+        return side if q == 0 else 1 - side
 
     def own(value):
         return jnp.where(top == 0, value[:own_rows], value[HALO:])
@@ -373,7 +382,7 @@
         return remote(tot.at[p, rows], from_in.at[p, rows], b_send.at[0], in_recv.at[s], {"rep": outward})
 
     def piece_rows(base, h):
-        if isinstance(base, int):
+        if isinstance(base, int) and isinstance(h, int):
             return slice(base + h * LANES, base + (h + 1) * LANES)
         return pl.ds(pl.multiple_of(base + h * LANES, LANES), LANES)
 
@@ -381,7 +390,7 @@
         tensor, q = s // subs, s % subs
         slot = (s * per + h) % WIDE
         if tensor == 0:
-            dst = down_ref.at[piece_rows(c * cw, h), q * cw : (q + 1) * cw]
+            dst = down_ref.at[piece_rows(c * cw, hidden_side(q)), h * cw : (h + 1) * cw]
         elif tensor == 1:
             dst = gate_ref.at[piece_rows(q * cw, h), chunk_cols(c)]
         else:
@@ -405,8 +414,8 @@
             lanes = lanes + square[:, g * LANES : (g + 1) * LANES]
         row = jnp.sum(lanes.T, axis=0, keepdims=True)
         if tensor == 0:
-            at = pl.ds(c * per + h, 1)
-            rows_d[at, :] = row if q == 0 else rows_d[at, :] + row
+            at = pl.ds(c * per + hidden_side(q), 1)
+            rows_d[at, :] = row if h == 0 else rows_d[at, :] + row
         else:
             at = ((tensor - 1) * subs + q) * per + h
             rows_gu[at : at + 1, :] = rows_gu[at : at + 1, :] + row
@@ -450,10 +459,20 @@
     def work(c, s):
         tensor, q = s // subs, s % subs
         p = c * slots + s
-        if q == 0:
-            gathered(c, tensor)
+
+        def middle(h):
+            ca, sa, ha, ka = behind(c, s, h, A_LAG)
+            guarded(c, ka, functools.partial(stage_a, ca * slots + sa, ha))
+            cb, sb, hb, kb = behind(c, s, h, B_LAG)
+            guarded(c, kb, functools.partial(stage_b, cb, sb, hb))
+
+        if not isinstance(c, int) or c > 0 or s > 0:
+            pl.when(is_mid)(lambda: middle(0))
+        gathered(c, tensor, q)
         if tensor == 0:
-            value = jnp.dot(h_all[c], og_ref[:, q * cw : (q + 1) * cw], preferred_element_type=f32)
+            rows = pl.ds(pl.multiple_of(hidden_side(q) * LANES, LANES), LANES)
+            value = jnp.dot(h_all[c, rows, :], og_ref[...], preferred_element_type=f32)
+            value = jnp.concatenate([value[:, n * cw : (n + 1) * cw] for n in range(subs)], axis=0)
         elif tensor == 1:
             value = jnp.dot(xt[q], g_all[c], preferred_element_type=f32)
         else:
@@ -471,11 +490,7 @@
         @pl.when(is_mid)
         def _():
             ring[lax.rem(p, RING)] = value
-            for h in range(per):
-                ca, sa, ha, ka = behind(c, s, h, A_LAG)
-                guarded(c, ka, functools.partial(stage_a, ca * slots + sa, ha))
-                cb, sb, hb, kb = behind(c, s, h, B_LAG)
-                guarded(c, kb, functools.partial(stage_b, cb, sb, hb))
+            middle(1)
 
     def input_term(c):
         cols = chunk_cols(c)
@@ -564,9 +579,8 @@
 
     def body(c, last=False):
         for s in range(slots):
-            if s > 0 or not isinstance(c, int) or c > 0:
-                for step in STEPS[s]:
-                    run(step, c)
+            for step in (FIRST_STEPS if isinstance(c, int) and c == 0 else STEPS)[s]:
+                run(step, c)
             if last and s == 1:
                 for copy in tap_peers:
                     copy.start()
@@ -583,27 +597,31 @@
     loads[2].wait()
     product(0, 1)
     pl.semaphore_wait(barrier, n_fs + 1 + jnp.where(is_mid, 1, 0))
+    pl.when(t == 1)(lambda: pl.semaphore_wait(go_sem, 1))
     reduce_send(0, 0)
     reduce_send(0, 1)
     loads[3].wait()
     loads[4].wait()
-    product(0, 2)
+    reduce_start(0, 2)
     for q in range(subs):
         xt[q] = x_ref[:, q * cw : (q + 1) * cw].astype(f32).T.astype(bf16)
     rows_gu[...] = jnp.zeros_like(rows_gu)
     for copy in loads[5:]:
         copy.wait()
     combine(0, 0)
+
+    @pl.when(t == 0)
+    def _():
+        pl.semaphore_signal(go_sem, inc=1, device_id={"tp": 1 - t}, device_id_type=MESH_ID)
+
     combine(0, 1)
-    reduce_send(0, 2)
-    if chunks > 1:
-        product(1, 0)
+    product(1, 0)
+    combine(0, 2)
     hidden_step(0)
-    combine(0, 2)
     grads_step(0)
     gather_start(0, 1)
-    if chunks > 1:
-        reduce_send(1, 0)
+    reduce_send(1, 0)
+    reduce_start(1, 1)
     body(0)
 
     @pl.loop(1, chunks - 1)
@@ -654,9 +672,12 @@
     for n in range(6):
         rows = halves[n % 2]
         all_sent(recv_part.at[:, :, n, 0 : rows.stop - rows.start], rs_send.at[n])
-    columns = h_all.shape[1]
-    for slot, quarters in ((0, 12), (1, 12), (2, 10), (3, 2)):
-        all_sent(h_all.at[:, 0 : columns * quarters // 16], ag_send.at[slot])
+    blocks = chunks * 3
+    for slot in range(2):
+        all_sent(part.at[0:blocks, 0 : own_rows // 2], ag_send.at[slot])
+    for slot in range(2, 4):
+        all_sent(part.at[0 : blocks - 2, 0 : own_rows // 4], ag_send.at[slot])
+    all_sent(part.at[0:2, 0 : own_rows // 2], ag_send.at[4])
     all_sent(part, a_send.at[0])
     tap_part.wait_send()
 
@@ -685,21 +706,25 @@
 def finish_kernel(
     gate, up, down, in_grad, taps, rows_gu, rows_d,
     gate_out, up_out, down_out, in_grad_out, taps_out, rows_gate_out, rows_up_out, rows_down_out,
-    sems,
+    rows_gate, rows_up, rows_down, sems,
 ):
     copies = []
-    for src, dst in ((gate, gate_out), (up, up_out), (down, down_out)):
+
+    def send(src, dst):
         copy = pltpu.make_async_copy(src, dst, sems.at[len(copies)])
         copy.start()
         copies.append(copy)
-    in_grad_out[...] = in_grad[...]
-    taps_out[...] = taps[...]
-    groups = rows_gate_out.shape[0] // LANES
+
+    for src, dst in ((gate, gate_out), (up, up_out), (down, down_out), (in_grad, in_grad_out), (taps, taps_out)):
+        send(src, dst)
+    groups = rows_gate.shape[0] // LANES
     for i in range(groups):
-        rows_gate_out[pl.ds(i * LANES, LANES)] = rows_gu[i]
-        rows_up_out[pl.ds(i * LANES, LANES)] = rows_gu[groups + i]
-    for i in range(rows_down_out.shape[0] // LANES):
-        rows_down_out[pl.ds(i * LANES, LANES)] = rows_d[i]
+        rows_gate[pl.ds(i * LANES, LANES)] = rows_gu[i]
+        rows_up[pl.ds(i * LANES, LANES)] = rows_gu[groups + i]
+    for i in range(rows_down.shape[0] // LANES):
+        rows_down[pl.ds(i * LANES, LANES)] = rows_d[i]
+    for src, dst in ((rows_gate, rows_gate_out), (rows_up, rows_up_out), (rows_down, rows_down_out)):
+        send(src, dst)
     for copy in copies:
         copy.wait()
 
@@ -782,8 +807,8 @@
             local((chunks * per, LANES), f32),
             local((2 * subs * per, LANES), f32),
             local((n_fs - 1, chunks * per, LANES), f32),
-            dma((6,)), dma((36,)), dma((4,)), dma((24,)),
-            dma((1,)), dma((KEEP,)), dma((KEEP,)), dma((1,)), dma((WIDE,)), dma((4,)), dma((8,)),
+            dma((6,)), dma((36,)), dma((5,)), dma((24,)),
+            dma((1,)), dma((KEEP,)), dma((KEEP,)), dma((1,)), dma((WIDE,)), dma((4,)), dma((8,)), pltpu.SemaphoreType.REGULAR,
             dma((4 * (n_fs - 1) + 8,)),
         ],
         compiler_params=pltpu.CompilerParams(
@@ -797,9 +822,9 @@
             whole((tok // 2, feat), bf16), whole((KW, hid), f32),
             whole((feat,), f32), whole((feat,), f32), whole((hid,), f32),
         ),
-        in_specs=[anywhere] * 3 + [vmem] * 4,
-        out_specs=(anywhere,) * 3 + (vmem,) * 5,
-        scratch_shapes=[dma((3,))],
+        in_specs=[anywhere] * 5 + [vmem] * 2,
+        out_specs=(anywhere,) * 8,
+        scratch_shapes=[local((feat,), f32), local((feat,), f32), local((hid,), f32), dma((8,))],
         compiler_params=pltpu.CompilerParams(vmem_limit_bytes=24 * 1024 * 1024),
     )(gate, up, down, in_grad, taps, rows_gu, rows_d)
     return (in_grad, gate, up, down, taps, rows_gate, rows_up, rows_down)

time: 142 us -> 137 us (0.965)
  Pallas kernels: 141 us -> 136 us
    pallas_call x1, Pallas kernels: 136 us -> 132 us  [fused_shards(): pl.pallas_call(functools.partial(layer_kernel, n_rep, n_fs), out_shape=(l...]
where the time goes in v3:
time: 137 us
  Pallas kernels  136 us (99%)
    pallas_call x1, Pallas kernels, fused_shards(): pl.pallas_call(functools.partial(layer_kernel, n_rep, n_fs), out_shape=(l...  132 us
    pallas_call x1, Pallas kernels, fused_shards(): pl.pallas_call(finish_kernel, out_shape=(whole((feat, hid), f32), whole((...  3.82 us

profile of v3, /device:TPU:0, one launch (start us, length us, event | category | flops | bytes accessed | tf_op | source)
XLA Modules:
  0.0 136.9 jit_solution(7146823454339284586)
XLA Ops:
  0.6 132.3 %shard_map.125 = (bf16[256,512]{1,0:T(8,128)(2,1)S(1)}, f32[1536,512]{1,0:T(8,128)S(1)}, f32[512,1536]{1,0:T(8,128)S(1)}, f32[512,1536]{1,0:T(8,128)S(1)}, f32[3...) custom-call(bf16[512,512]{1,0:T(8,128)(2,1)} %x_hbm.1, bf16[512,1536]{1,0:T(8,128)(2,1)} %wg_hbm.1, ...), custom_call_target="tpu_custom_call" | custom-call | tf_op jit(solution)/shard_map/pallas_call | solution.py:761
  132.9 3.8 %shard_map.126 = (f32[512,1536]{1,0:T(8,128)}, f32[512,1536]{1,0:T(8,128)}, f32[1536,512]{1,0:T(8,128)}, bf16[256,512]{1,0:T(8,128)(2,1)}, f32[3,1536]{1,0:T(4,1...) custom-call(f32[512,1536]{1,0:T(8,128)S(1)} %get-tuple-element.23.gate, f32[512,1536]{1,0:T(8,128)S(1)} %get-tuple-element.24.up, ...), custom_call_target="tpu_custom_call" | custom-call | tf_op jit(solution)/shard_map/pallas_call | solution.py:818

commit v4 on v3

--- a/solution.py
+++ b/solution.py
@@ -117,9 +117,9 @@
 
 def layer_kernel(
     n_rep, n_fs,
-    x_hbm, wg_hbm, wu_hbm, taps_ref, wd_hbm, og_hbm,
+    x_hbm, wg_hbm, wu_hbm, taps_hbm, wd_hbm, og_hbm,
     in_grad_out, down_ref, gate_ref, up_ref, taps_out, rows_gu_out, rows_down_out,
-    x_ref, wg_ref, wu_ref, wd_ref, og_ref,
+    x_ref, wg_ref, wu_ref, taps_ref, wd_ref, og_ref,
     xt, send_part, recv_part, pair_part, held, h_all, g_all, u_all, ring, wide, part, from_out, from_in, tot,
     acc, ig_send, ig_recv, in_grad_ref, taps_out_ref, rows_gu_ref, rows_down_ref, tap_all, tap_two, tap_out, tap_in, tap_sum, rows_gu, rows_d, rows_tp, rows_fs,
     rs_send, rs_recv, ag_send, ag_recv, a_send, out_recv, in_recv, b_send, wide_sem, out_sem, loc_sem, go_sem, misc,
@@ -175,6 +175,7 @@
     load(wu_hbm.at[:, first], wu_ref.at[:, first])
     load(og_hbm, og_ref)
     load(wd_hbm.at[first], wd_ref.at[first])
+    load(taps_hbm, taps_ref)
     if chunks > 1:
         rest = slice(cw, chunks * cw)
         load(wg_hbm.at[:, rest], wg_ref.at[:, rest])
@@ -225,8 +226,8 @@
             lane = (g % 2) * LANES
             send_part[c, tensor, g] = value[row : row + span, lane : lane + LANES]
 
-    def reduce_send(c, tensor):
-        for n in range(4):
+    def reduce_send(c, tensor, steps=range(4)):
+        for n in steps:
             rs_copy(c, tensor, n).start()
 
     def reduce_start(c, tensor):
@@ -594,12 +595,14 @@
     loads[0].wait()
     loads[1].wait()
     product(0, 0)
+    pl.semaphore_wait(barrier, n_fs + 1 + jnp.where(is_mid, 1, 0))
+    pl.when(t == 1)(lambda: pl.semaphore_wait(go_sem, 1))
+    reduce_send(0, 0, range(2))
     loads[2].wait()
     product(0, 1)
-    pl.semaphore_wait(barrier, n_fs + 1 + jnp.where(is_mid, 1, 0))
-    pl.when(t == 1)(lambda: pl.semaphore_wait(go_sem, 1))
-    reduce_send(0, 0)
-    reduce_send(0, 1)
+    reduce_send(0, 1, range(2))
+    reduce_send(0, 0, range(2, 4))
+    reduce_send(0, 1, range(2, 4))
     loads[3].wait()
     loads[4].wait()
     reduce_start(0, 2)
@@ -769,12 +772,13 @@
             local((2 * subs * per, LANES), f32),
             local((chunks * per, LANES), f32),
         ),
-        in_specs=[hbm, hbm, hbm, vmem, hbm, hbm],
+        in_specs=[hbm] * 6,
         out_specs=(anywhere,) * 7,
         scratch_shapes=[
             local((tok, feat), bf16),
             local((feat, hid), bf16),
             local((feat, hid), bf16),
+            local((KW, hid), bf16),
             local((hid, feat), bf16),
             local((tok, feat), bf16),
             local((subs, cw, tok), bf16),
@@ -808,7 +812,7 @@
             local((2 * subs * per, LANES), f32),
             local((n_fs - 1, chunks * per, LANES), f32),
             dma((6,)), dma((36,)), dma((5,)), dma((24,)),
-            dma((1,)), dma((KEEP,)), dma((KEEP,)), dma((1,)), dma((WIDE,)), dma((4,)), dma((8,)), pltpu.SemaphoreType.REGULAR,
+            dma((1,)), dma((KEEP,)), dma((KEEP,)), dma((1,)), dma((WIDE,)), dma((4,)), dma((9,)), pltpu.SemaphoreType.REGULAR,
             dma((4 * (n_fs - 1) + 8,)),
         ],
         compiler_params=pltpu.CompilerParams(

time: 137 us -> 136 us (level)
  no operation moved by 1% of the time
where the time goes in v4:
time: 136 us
  Pallas kernels  135 us (99%)
    pallas_call x1, Pallas kernels, fused_shards(): pl.pallas_call(functools.partial(layer_kernel, n_rep, n_fs), out_shape=(l...  132 us
    pallas_call x1, Pallas kernels, fused_shards(): pl.pallas_call(finish_kernel, out_shape=(whole((feat, hid), f32), whole((...  3.82 us

profile of v4, /device:TPU:0, one launch (start us, length us, event | category | flops | bytes accessed | tf_op | source)
XLA Modules:
  0.0 136.1 jit_solution(5738002790221474452)
XLA Ops:
  0.6 131.5 %shard_map.125 = (bf16[256,512]{1,0:T(8,128)(2,1)S(1)}, f32[1536,512]{1,0:T(8,128)S(1)}, f32[512,1536]{1,0:T(8,128)S(1)}, f32[512,1536]{1,0:T(8,128)S(1)}, f32[3...) custom-call(bf16[512,512]{1,0:T(8,128)(2,1)} %x_hbm.1, bf16[512,1536]{1,0:T(8,128)(2,1)} %wg_hbm.1, ...), custom_call_target="tpu_custom_call" | custom-call | tf_op jit(solution)/shard_map/pallas_call | solution.py:764
  132.1 3.8 %shard_map.126 = (f32[512,1536]{1,0:T(8,128)}, f32[512,1536]{1,0:T(8,128)}, f32[1536,512]{1,0:T(8,128)}, bf16[256,512]{1,0:T(8,128)(2,1)}, f32[3,1536]{1,0:T(4,1...) custom-call(f32[512,1536]{1,0:T(8,128)S(1)} %get-tuple-element.23.gate, f32[512,1536]{1,0:T(8,128)S(1)} %get-tuple-element.24.up, ...), custom_call_target="tpu_custom_call" | custom-call | tf_op jit(solution)/shard_map/pallas_call | solution.py:822

commit v5 on v4

--- a/solution.py
+++ b/solution.py
@@ -457,18 +457,17 @@
         else:
             pl.when(c >= lowest)(fn)
 
+    def middle_steps(c, s, h):
+        ca, sa, ha, ka = behind(c, s, h, A_LAG)
+        guarded(c, ka, functools.partial(stage_a, ca * slots + sa, ha))
+        cb, sb, hb, kb = behind(c, s, h, B_LAG)
+        guarded(c, kb, functools.partial(stage_b, cb, sb, hb))
+
     def work(c, s):
         tensor, q = s // subs, s % subs
         p = c * slots + s
 
-        def middle(h):
-            ca, sa, ha, ka = behind(c, s, h, A_LAG)
-            guarded(c, ka, functools.partial(stage_a, ca * slots + sa, ha))
-            cb, sb, hb, kb = behind(c, s, h, B_LAG)
-            guarded(c, kb, functools.partial(stage_b, cb, sb, hb))
-
-        if not isinstance(c, int) or c > 0 or s > 0:
-            pl.when(is_mid)(lambda: middle(0))
+        middle = functools.partial(middle_steps, c, s)
         gathered(c, tensor, q)
         if tensor == 0:
             rows = pl.ds(pl.multiple_of(hidden_side(q) * LANES, LANES), LANES)
@@ -580,6 +579,8 @@
 
     def body(c, last=False):
         for s in range(slots):
+            if not isinstance(c, int) or c > 0 or s > 0:
+                pl.when(is_mid)(functools.partial(middle_steps, c, s, 0))
             for step in (FIRST_STEPS if isinstance(c, int) and c == 0 else STEPS)[s]:
                 run(step, c)
             if last and s == 1:

time: 136 us -> 136 us (level)
  no operation moved by 1% of the time
where the time goes in v5:
time: 136 us
  Pallas kernels  135 us (99%)
    pallas_call x1, Pallas kernels, fused_shards(): pl.pallas_call(functools.partial(layer_kernel, n_rep, n_fs), out_shape=(l...  131 us
    pallas_call x1, Pallas kernels, fused_shards(): pl.pallas_call(finish_kernel, out_shape=(whole((feat, hid), f32), whole((...  3.82 us

profile of v5, /device:TPU:0, one launch (start us, length us, event | category | flops | bytes accessed | tf_op | source)
XLA Modules:
  0.0 136.0 jit_solution(18397938468964668609)
XLA Ops:
  0.6 131.4 %shard_map.125 = (bf16[256,512]{1,0:T(8,128)(2,1)S(1)}, f32[1536,512]{1,0:T(8,128)S(1)}, f32[512,1536]{1,0:T(8,128)S(1)}, f32[512,1536]{1,0:T(8,128)S(1)}, f32[3...) custom-call(bf16[512,512]{1,0:T(8,128)(2,1)} %x_hbm.1, bf16[512,1536]{1,0:T(8,128)(2,1)} %wg_hbm.1, ...), custom_call_target="tpu_custom_call" | custom-call | tf_op jit(solution)/shard_map/pallas_call | solution.py:765
  132.0 3.8 %shard_map.126 = (f32[512,1536]{1,0:T(8,128)}, f32[512,1536]{1,0:T(8,128)}, f32[1536,512]{1,0:T(8,128)}, bf16[256,512]{1,0:T(8,128)(2,1)}, f32[3,1536]{1,0:T(4,1...) custom-call(f32[512,1536]{1,0:T(8,128)S(1)} %get-tuple-element.23.gate, f32[512,1536]{1,0:T(8,128)S(1)} %get-tuple-element.24.up, ...), custom_call_target="tpu_custom_call" | custom-call | tf_op jit(solution)/shard_map/pallas_call | solution.py:823
